TPU v7x, 32 devices: a whole 2x2x4 slice. The times are simulated.
32 devices in a mesh: sp: 8 (over z, y), tp: 4 (over x, core).
Axes of the slice: x: 2, y: 2, z: 4, core: 2. Of those that a mesh axis runs over, the one named last changes fastest.
Arguments:
- tokens: bfloat16 [2560, 2048], P('sp', 'tp'), may hold values from -6 to 6
- pre_gain: float32 [2, 2048], replicated, may hold values from 0.1 to 1.9
- w_value: bfloat16 [2, 2048, 2048], P(None, 'sp', 'tp'), may hold values from -0.125 to 0.125
- w_gate: bfloat16 [2, 2048, 2048], P(None, 'sp', 'tp'), may hold values from -0.125 to 0.125
- taps: float32 [2, 31, 2048], P(None, None, 'tp'), may hold values from -5 to 5
- norm_gain: float32 [2, 2048], P(None, 'tp'), may hold values from 0.1 to 1.9
- norm_shift: float32 [2, 2048], P(None, 'tp'), may hold values from -3 to 3
- w_out: bfloat16 [2, 2048, 2048], P(None, 'tp', 'sp'), may hold values from -2 to 2
- post_gain: float32 [2, 2048], P(None, 'tp'), may hold values from 0.1 to 1.9
Outputs:
- stream: bfloat16 [2560, 2048], P('sp', 'tp')
All inputs are finite; a program needn't handle non-finite values.
Results may differ from a plain program's by a relative error of at most 0.015.
Values may be sent and summed in bfloat16 or wider, within the bound.
A program may use at most 64 MiB of HBM per device.

v0:
```python
import functools

import jax
import jax.numpy as jnp
from jax import lax
from jax.experimental import pallas as pl
from jax.experimental.pallas import tpu as pltpu
from jax.sharding import PartitionSpec as P

D = 2048
CONV_WIDTH = 31
LAYERS = 2


EPSILON = 1e-06
LN_EPSILON = 1e-05


def passed_along(block, axis, distance):
    devices = range(lax.axis_size(axis))
    route = [(i - distance, i) for i in devices if i - distance in devices]
    return lax.ppermute(block, axis, route)


def local(tokens, pre_gain, w_value, w_gate, taps, norm_gain, norm_shift, w_out, post_gain):
    stream = tokens
    full_value, full_gate = (
        lax.all_gather(w_value, "sp", axis=1, tiled=True),
        lax.all_gather(w_gate, "sp", axis=1, tiled=True),
    )
    full_out = lax.all_gather(w_out, "sp", axis=2, tiled=True)
    for layer in range(LAYERS):
        whole = lax.all_gather(stream, "tp", axis=1, tiled=True)
        whole_f = whole.astype(jnp.float32)
        normed = (
            whole_f
            * lax.rsqrt(jnp.mean(whole_f * whole_f, -1, keepdims=True) + EPSILON)
            * pre_gain[layer]
        ).astype(jnp.bfloat16)
        value_mat = full_value[layer]
        gate_mat = full_gate[layer]
        out_mat = full_out[layer]
        value_proj = jnp.dot(normed, value_mat, preferred_element_type=jnp.float32)
        gate_proj = jnp.dot(normed, gate_mat, preferred_element_type=jnp.float32)
        glu_act = (value_proj * jax.nn.sigmoid(gate_proj)).astype(jnp.bfloat16)
        rows = glu_act.shape[0]
        fringe = passed_along(glu_act[rows - (CONV_WIDTH - 1) :], "sp", 1)
        padded = jnp.concatenate([fringe, glu_act], 0).astype(jnp.float32)
        conv_out = jnp.zeros(glu_act.shape, jnp.float32)
        for offset in range(CONV_WIDTH):
            conv_out = conv_out + taps[layer, offset] * padded[offset : offset + rows]
        row_sum, row_square = lax.psum(
            (jnp.sum(conv_out, -1, keepdims=True), jnp.sum(conv_out * conv_out, -1, keepdims=True)),
            "tp",
        )
        center = row_sum / D
        spread = jnp.maximum(row_square / D - center * center, 0.0)
        activated = jax.nn.silu(
            (conv_out - center) * lax.rsqrt(spread + LN_EPSILON) * norm_gain[layer]
            + norm_shift[layer]
        ).astype(jnp.bfloat16)
        terms = jnp.dot(activated, out_mat, preferred_element_type=jnp.float32)
        summed = lax.psum_scatter(terms.astype(jnp.bfloat16), "tp", scatter_dimension=1, tiled=True)
        projected = summed.astype(jnp.float32)
        out_square = lax.psum(jnp.sum(projected * projected, -1, keepdims=True), "tp")
        scale = lax.rsqrt(out_square / D + EPSILON)
        stream = (stream.astype(jnp.float32) + projected * scale * post_gain[layer]).astype(
            jnp.bfloat16
        )
    return stream


TILE = 64
PACK = 16
HALO = 32


def step(
    nz, x_ref, pre_ref, wv_hbm, wg_hbm, taps_ref, ng_ref, ns_ref, wo_hbm, post_ref, out_ref,
    wvg, other, wo, whole, normed, glu, conv, act, act_out, part_out, part_in, cross_out, cross_in,
    total, taps, gain, shift, stat, stat_in, local_sem,
    su, ru, sd, rd, ys, yr, gs, gr, hs, hr, ss, sr, ps, pr, cs, cr, acs, acr,
):
    sp, tp = lax.axis_index("sp"), lax.axis_index("tp")
    nsp, ntp = 2 * nz, 4
    z, y = sp // 2, sp % 2
    x, c = tp // 2, tp % 2
    up, down, beside = (sp + 2, tp), (sp - 2, tp), (z * 2 + 1 - y, tp)
    mate, across, diagonal = (sp, x * 2 + 1 - c), (sp, (1 - x) * 2 + c), (sp, (1 - x) * 2 + 1 - c)
    rows, cols = x_ref.shape
    layers = pre_ref.shape[0]
    units = 3 * layers
    both, half = 2 * rows, cols // 2
    twice = [u for u in range(units) if u % 3 < 2]
    mine = pl.ds(pl.multiple_of(y * half, half), half)

    def copy(src, dst, send, recv, to):
        return pltpu.make_async_remote_copy(
            src_ref=src, dst_ref=dst, send_sem=send, recv_sem=recv, device_id=to,
            device_id_type=pl.DeviceIdType.MESH,
        )

    def piece(u, slot):
        l, kind = divmod(u, 3)
        if kind < 2:
            depth = wv_hbm.shape[1]
            return wvg.at[2 * l + kind, pl.ds(pl.multiple_of(slot * depth, depth), depth)]
        depth = wo_hbm.shape[1]
        return wo.at[l, pl.ds(pl.multiple_of(slot * depth, depth), depth)]

    def lanes(u, yy):
        return u + sum(t < u for t in twice) + yy

    def sides(u):
        return (0, 1) if u in twice else (0,)

    def up_copy(u, yy, k):
        i, p = lanes(u, yy), piece(u, (z - k) * 2 + (1 - y if yy else y))
        return copy(p, p, su.at[i, k], ru.at[i, k], up)

    def down_copy(u, yy, k):
        i, p = lanes(u, yy), piece(u, (z + k) * 2 + (1 - y if yy else y))
        return copy(p, p, sd.at[i, k], rd.at[i, k], down)

    def beside_copy(u, oz):
        p = piece(u, oz * 2 + y)
        if u in twice:
            l, kind = divmod(u, 3)
            return copy(other.at[2 * l + kind], p, ys.at[u, oz], yr.at[u, oz], beside)
        return copy(p, p, ys.at[u, oz], yr.at[u, oz], beside)

    def beside_wait(u, oz):
        p = piece(u, oz * 2 + 1 - y)
        copy(p, p, ys.at[u, oz], yr.at[u, oz], beside).wait_recv()

    def along(u, yy):
        pl.when(z + 1 < nz)(lambda: up_copy(u, yy, 0).start())
        pl.when(z > 0)(lambda: down_copy(u, yy, 0).start())

    def own(u):
        along(u, 0)
        beside_copy(u, z).start()

    def own_second(u):
        beside_wait(u, z)
        along(u, 1)

    def relay(u, d):
        for yy in sides(u):
            i = lanes(u, yy)
            side = 1 - y if yy else y

            @pl.when(z >= d)
            def _():
                p = piece(u, (z - d) * 2 + side)
                copy(p, p, su.at[i, d], ru.at[i, d - 1], beside).wait_recv()
                pl.when(z + 1 < nz)(lambda: up_copy(u, yy, d).start())
                if u not in twice:
                    beside_copy(u, z - d).start()

            @pl.when(z + d < nz)
            def _():
                p = piece(u, (z + d) * 2 + side)
                copy(p, p, sd.at[i, d], rd.at[i, d - 1], beside).wait_recv()
                pl.when(z > 0)(lambda: down_copy(u, yy, d).start())
                if u not in twice:
                    beside_copy(u, z + d).start()

    def arrive(u):
        if u not in twice:
            for oz in range(nz):
                beside_wait(u, oz)

    def sent():
        for u in range(units):
            for yy in sides(u):
                for k in range(nz - 1):
                    pl.when((z >= k) & (z + 1 < nz))(lambda: up_copy(u, yy, k).wait_send())
                    pl.when((z + k < nz) & (z > 0))(lambda: down_copy(u, yy, k).wait_send())
            if u in twice:
                beside_copy(u, z).wait_send()
            else:
                for oz in range(nz):
                    beside_copy(u, oz).wait_send()

    here, there = y * 4, (1 - y) * 4
    opposite = (1 - x) * 2 + c

    routes = dict(
        across=(here + tp, across),
        beside=(here + tp, beside),
        mate=(here + tp, mate),
        across_mate=(here + opposite, mate),
        beside_across=(there + tp, across),
        beside_mate=(there + tp, mate),
        both_mate=(there + opposite, mate),
        across_beside=(here + opposite, beside),
    )
    upper, lower = pl.ds(0, rows // 2), pl.ds(rows // 2, rows // 2)
    parts = dict(beside_across=upper, across_beside=lower)

    def gather(l, name):
        k = list(routes).index(name)
        t, to = routes[name]
        b = whole.at[l, t, parts[name]] if name in parts else whole.at[l, t]
        return copy(b, b, gs.at[l, k], gr.at[l, k], to)

    def came(l, k, t, part=pl.ds(0, rows)):
        b = whole.at[l, t, part]
        copy(b, b, gs.at[l, k], gr.at[l, k], mate).wait_recv()

    def gather_start(l):
        for name in ("across", "beside", "mate"):
            gather(l, name).start()

    def gather_turn(l):
        came(l, 1, there + tp)
        gather(l, "beside_across").start()
        gather(l, "beside_mate").start()
        came(l, 0, here + opposite)
        gather(l, "across_beside").start()
        gather(l, "across_mate").start()

    def gather_last(l):
        came(l, 4, there + opposite, upper)
        came(l, 7, there + opposite, lower)
        gather(l, "both_mate").start()

    def gather_wait(l):
        pair_tp, pair_opposite = x * 2 + 1 - c, (1 - x) * 2 + 1 - c
        came(l, 2, here + pair_tp)
        came(l, 3, here + pair_opposite)
        came(l, 5, there + pair_tp)
        came(l, 6, there + pair_opposite)

    def norm(l):
        gather_wait(l)
        tiles = rows // TILE

        @pl.loop(0, 2 * tiles)
        def _(i):
            g, r = i // tiles * 4, pl.ds(pl.multiple_of(i % tiles * TILE, TILE), TILE)
            to = pl.ds(pl.multiple_of(i * TILE, TILE), TILE)
            square = jnp.zeros((TILE, 1), jnp.float32)
            for t in range(ntp):
                v = whole[l, g + t, r, :].astype(jnp.float32)
                square = square + jnp.sum(v * v, -1, keepdims=True)
            scale = lax.rsqrt(square / (cols * ntp) + EPSILON)
            for t in range(ntp):
                v = whole[l, g + t, r, :].astype(jnp.float32)
                at = slice(t * cols, (t + 1) * cols)
                normed[to, at] = (v * scale * pre_ref[l : l + 1, at]).astype(jnp.bfloat16)

    def halo(l):
        return copy(
            glu.at[l, pl.ds(both, HALO)], glu.at[l, pl.ds(0, HALO)], hs.at[l], hr.at[l], up
        )

    def project(l):
        n = normed[...]
        value = jnp.dot(n, wvg[2 * l], preferred_element_type=jnp.float32)
        gate = jnp.dot(n, wvg[2 * l + 1], preferred_element_type=jnp.float32)
        glu[l, HALO:, :] = (value * jax.nn.sigmoid(gate)).astype(jnp.bfloat16)
        pl.when(z + 1 < nz)(lambda: halo(l).start())

    partner = z * 2 + 1 - y
    peers = [mate, across, diagonal, beside]
    peers += [(partner, mate[1]), (partner, across[1]), (partner, diagonal[1])]

    def exchange(e):
        return [
            copy(stat.at[e], stat_in.at[e, j], ss.at[e, j], sr.at[e, j], to)
            for j, to in enumerate(peers[: 3 if e % 2 else 7])
        ]

    def exchanged(e):
        sums = stat[e]
        for j, s in enumerate(exchange(e)):
            s.wait_recv()
            sums = sums + stat_in[e, j]
        return sums

    lane = lax.broadcasted_iota(jnp.int32, (PACK, 128), 1)
    groups = TILE // PACK

    def pick(sums, at):
        found = [
            jnp.sum(jnp.where(lane == at * groups + g, sums, 0.0), -1, keepdims=True)
            for g in range(groups)
        ]
        return jnp.concatenate(found, 0)

    def pack(sums, at, column):
        for g in range(groups):
            sums = jnp.where(lane == at * groups + g, column[g * PACK : (g + 1) * PACK], sums)
        return sums

    def convolve(l):
        @pl.when(z == 0)
        def _():
            glu[l, :HALO] = jnp.zeros((HALO, half), jnp.bfloat16)

        pl.when(z > 0)(lambda: halo(l).wait_recv())
        first = HALO - (CONV_WIDTH - 1)

        def tile(i, sums):
            r = pl.multiple_of(i * TILE, TILE)
            one = jnp.zeros((TILE, 128), jnp.float32)
            two = jnp.zeros((TILE, 128), jnp.float32)
            for j in range(half // 128):
                at = slice(j * 128, (j + 1) * 128)
                window = glu[l, pl.ds(r, TILE + HALO), at].astype(jnp.float32)
                acc = jnp.zeros((TILE, 128), jnp.float32)
                for s in range(8):
                    w = window if s == 0 else pltpu.roll(window, TILE + HALO - s, 0)
                    for k in range(CONV_WIDTH):
                        if (first + k) % 8 == s:
                            o = first + k - s
                            acc = acc + taps[l, k : k + 1, at] * w[o : o + TILE]
                conv[pl.ds(r, TILE), at] = acc
                one = one + acc
                two = two + acc * acc
            sums = pack(sums, 2 * i, jnp.sum(one, -1, keepdims=True))
            return pack(sums, 2 * i + 1, jnp.sum(two, -1, keepdims=True))

        stat[2 * l] = lax.fori_loop(0, both // TILE, tile, jnp.zeros((PACK, 128), jnp.float32))
        for s in exchange(2 * l):
            s.start()

    def activate(l):
        sums = exchanged(2 * l)
        tiles = rows // TILE

        def tile(q, i, store):
            at = q * tiles + i
            r = pl.ds(pl.multiple_of(at * TILE, TILE), TILE)
            center = pick(sums, 2 * at) / (cols * ntp)
            spread = jnp.maximum(pick(sums, 2 * at + 1) / (cols * ntp) - center * center, 0.0)
            v = (conv[r, :] - center) * lax.rsqrt(spread + LN_EPSILON)
            v = v * gain[l : l + 1, :] + shift[l : l + 1, :]
            store(pl.ds(pl.multiple_of(i * TILE, TILE), TILE), (v * jax.nn.sigmoid(v)).astype(jnp.bfloat16))

        def give_away(r, v):
            act_out[l, r, :] = v

        def keep(r, v):
            act[l, y, r, :] = v

        pl.loop(0, tiles)(lambda i: tile(1 - y, i, give_away))
        shared(l).start()
        pl.loop(0, tiles)(lambda i: tile(y, i, keep))
        b = act.at[l, 1 - y]
        copy(b, b, acs.at[l], acr.at[l], beside).wait_recv()

    def shared(l):
        return copy(act_out.at[l], act.at[l, y], acs.at[l], acr.at[l], beside)

    each = wo_hbm.shape[2]
    per = cols // each
    depth = wo_hbm.shape[1]

    def term(l, t, h):
        w = wo[l, pl.ds(pl.multiple_of((t * per + h) * depth, depth), depth), :]
        first = jnp.dot(act[l, 0], w[:half], preferred_element_type=jnp.float32)
        second = jnp.dot(act[l, 1], w[half:], preferred_element_type=jnp.float32)
        return (first + second).astype(jnp.bfloat16)

    def pair(l, far, h):
        i = far * per + h
        return copy(part_out.at[l, i], part_in.at[l, i], ps.at[l, i], pr.at[l, i], mate)

    def over(l, h):
        return copy(cross_out.at[l, h], cross_in.at[l, h], cs.at[l, h], cr.at[l, h], across)

    def give(l, far, h):
        t = ((1 - x) if far else x) * 2 + 1 - c
        part_out[l, far * per + h] = term(l, t, h)
        pair(l, far, h).start()

    def joined(l, far, h):
        t = ((1 - x) if far else x) * 2 + c
        kept = term(l, t, h).astype(jnp.float32)
        pair(l, far, h).wait_recv()
        return kept + part_in[l, far * per + h].astype(jnp.float32)

    def reduce(l):
        for h in range(per):
            give(l, 1, h)
        for h in range(per):
            cross_out[l, h] = joined(l, 1, h).astype(jnp.bfloat16)
            over(l, h).start()
        for h in range(per):
            give(l, 0, h)
        for h in range(per):
            total[:, h * each : (h + 1) * each] = joined(l, 0, h)

    def finish(l):
        for h in range(per):
            over(l, h).wait_recv()

        def tile(i, sums):
            r = pl.ds(pl.multiple_of(i * TILE, TILE), TILE)
            square = jnp.zeros((TILE, 1), jnp.float32)
            for h in range(per):
                at = slice(h * each, (h + 1) * each)
                p = total[r, at] + cross_in[l, h, r, :].astype(jnp.float32)
                p = p.astype(jnp.bfloat16).astype(jnp.float32)
                total[r, at] = p
                square = square + jnp.sum(p * p, -1, keepdims=True)
            return pack(sums, i, square)

        e = 2 * l + 1
        stat[e] = lax.fori_loop(0, rows // TILE, tile, jnp.zeros((PACK, 128), jnp.float32))
        for s in exchange(e):
            s.start()
        sums = exchanged(e)

        @pl.loop(0, rows // TILE)
        def _(i):
            r = pl.ds(pl.multiple_of(i * TILE, TILE), TILE)
            scale = lax.rsqrt(pick(sums, i) / (cols * ntp) + EPSILON)
            old = whole[l, here + tp, r, :].astype(jnp.float32)
            new = (old + total[r, :] * scale * post_ref[l : l + 1, :]).astype(jnp.bfloat16)
            if l + 1 < layers:
                whole[l + 1, here + tp, r, :] = new
            else:
                out_ref[r, :] = new

    held = [pltpu.make_async_copy(x_ref, whole.at[0, here + tp], local_sem.at[units])]
    for u in range(units):
        l, kind = divmod(u, 3)
        ref = (wv_hbm, wg_hbm, wo_hbm)[kind]
        if kind < 2:
            part = ref.at[l, :, mine]
            rest = ref.at[l, :, pl.ds(pl.multiple_of((1 - y) * half, half), half)]
            i = 2 * l + kind
            held.append(pltpu.make_async_copy(rest, other.at[i], local_sem.at[units + 1 + i]))
        else:
            part = ref.at[l]
        held.append(pltpu.make_async_copy(part, piece(u, sp), local_sem.at[u]))
    for h in held:
        h.start()
    for l in range(layers):
        taps[l] = taps_ref[l, :, mine]
        gain[l : l + 1] = ng_ref[l : l + 1, mine]
        shift[l : l + 1] = ns_ref[l : l + 1, mine]
    barrier = pltpu.get_barrier_semaphore()
    for i in range(1, nsp):
        pl.semaphore_signal(
            barrier, inc=1, device_id=(lax.rem(sp + i, nsp), tp),
            device_id_type=pl.DeviceIdType.MESH,
        )
    for i in range(1, ntp):
        for at in (sp, partner):
            pl.semaphore_signal(
                barrier, inc=1, device_id=(at, lax.rem(tp + i, ntp)),
                device_id_type=pl.DeviceIdType.MESH,
            )
    pl.semaphore_wait(barrier, nsp - 1 + 2 * (ntp - 1))
    for h in held:
        h.wait()

    far = range(1, nz)
    gather_start(0)
    own(0)
    own(1)
    own_second(0)
    own_second(1)
    relay(0, 1)
    gather_turn(0)
    for d in far[1:]:
        relay(0, d)
    gather_last(0)
    own(2)
    relay(1, 1)
    norm(0)
    for d in far[1:]:
        relay(1, d)
    own(3)
    own_second(3)
    project(0)
    relay(2, 1)
    convolve(0)
    relay(2, 2)
    activate(0)
    for d in far[2:]:
        relay(2, d)
    own(4)
    own_second(4)
    relay(3, 1)
    arrive(2)
    reduce(0)
    relay(3, 2)
    for d in far[2:]:
        relay(3, d)
    own(5)
    finish(0)
    gather_start(1)
    relay(4, 1)
    gather_turn(1)
    relay(4, 2)
    for d in far[2:]:
        relay(4, d)
    gather_last(1)
    relay(5, 1)
    norm(1)
    project(1)
    relay(5, 2)
    convolve(1)
    for d in far[2:]:
        relay(5, d)
    activate(1)
    arrive(5)
    reduce(1)
    finish(1)

    sent()
    for l in range(layers):
        for name in routes:
            gather(l, name).wait_send()
        pl.when(z + 1 < nz)(lambda: halo(l).wait_send())
        shared(l).wait_send()
        for s in (*exchange(2 * l), *exchange(2 * l + 1)):
            s.wait_send()
        for h in range(per):
            over(l, h).wait_send()
            for side in (0, 1):
                pair(l, side, h).wait_send()


def kernel_local(nsp, *args):
    tokens, pre_gain, w_value, _, _, _, _, w_out, _ = args
    rows, cols = tokens.shape
    if rows % TILE or 4 * rows > PACK * 128:
        return local(*args)
    layers, depth = w_value.shape[:2]
    inner, each = w_out.shape[1:]
    nz, units, per = nsp // 2, 3 * layers, cols // each
    tracks, half = units + 2 * layers, cols // 2
    vmem, hbm = pl.BlockSpec(memory_space=pltpu.VMEM), pl.BlockSpec(memory_space=pl.ANY)
    bf16, f32, dma = jnp.bfloat16, jnp.float32, pltpu.SemaphoreType.DMA
    return pl.pallas_call(
        functools.partial(step, nz),
        out_shape=jax.ShapeDtypeStruct((rows, cols), bf16),
        in_specs=[hbm, vmem, hbm, hbm, vmem, vmem, vmem, hbm, vmem],
        out_specs=vmem,
        scratch_shapes=[
            pltpu.VMEM((2 * layers, nsp * depth, half), bf16),
            pltpu.VMEM((2 * layers, depth, half), bf16),
            pltpu.VMEM((layers, nsp * inner, each), bf16),
            pltpu.VMEM((layers, 8, rows, cols), bf16),
            pltpu.VMEM((2 * rows, 4 * cols), bf16),
            pltpu.VMEM((layers, HALO + 2 * rows, half), bf16),
            pltpu.VMEM((2 * rows, half), f32),
            pltpu.VMEM((layers, 2, rows, half), bf16),
            pltpu.VMEM((layers, rows, half), bf16),
            pltpu.VMEM((layers, 2 * per, rows, each), bf16),
            pltpu.VMEM((layers, 2 * per, rows, each), bf16),
            pltpu.VMEM((layers, per, rows, each), bf16),
            pltpu.VMEM((layers, per, rows, each), bf16),
            pltpu.VMEM((rows, cols), f32),
            pltpu.VMEM((layers, CONV_WIDTH, half), f32),
            pltpu.VMEM((layers, half), f32),
            pltpu.VMEM((layers, half), f32),
            pltpu.VMEM((2 * layers, PACK, 128), f32),
            pltpu.VMEM((2 * layers, 7, PACK, 128), f32),
            dma((units + 1 + 2 * layers,)),
            dma((tracks, nz)), dma((tracks, nz)), dma((tracks, nz)), dma((tracks, nz)),
            dma((units, nz)), dma((units, nz)),
            dma((layers, 8)), dma((layers, 8)),
            dma((layers,)), dma((layers,)),
            dma((2 * layers, 7)), dma((2 * layers, 7)),
            dma((layers, 2 * per)), dma((layers, 2 * per)),
            dma((layers, per)), dma((layers, per)),
            dma((layers,)), dma((layers,)),
        ],
        compiler_params=pltpu.CompilerParams(
            collective_id=0, has_side_effects=True, vmem_limit_bytes=56 * 1024 * 1024
        ),
    )(*args)


def solution(mesh):
    nsp, ntp = mesh.shape["sp"], mesh.shape["tp"]
    fits = nsp % 2 == 0 and 3 <= nsp // 2 <= 8 and ntp == 4 and D // max(nsp, 2 * ntp) % 128 == 0
    body = functools.partial(kernel_local, nsp) if fits else local
    placed = (
        P("sp", "tp"),
        P(),
        P(None, "sp", "tp"),
        P(None, "sp", "tp"),
        P(None, None, "tp"),
        P(None, "tp"),
        P(None, "tp"),
        P(None, "tp", "sp"),
        P(None, "tp"),
    )
    return jax.shard_map(
        body, mesh=mesh, in_specs=placed, out_specs=P("sp", "tp"), check_vma=False
    )
```

profile of v0, /device:TPU:0, one launch (start us, length us, event | category | flops | bytes accessed | tf_op | source)
XLA Modules:
  0.0 159.0 jit_solution(9726451933822765292)
XLA Ops:
  0.0 1.6 copy.10.taps_ref
  1.6 155.7 %shard_map.91 = bf16[320,512]{1,0:T(8,128)(2,1)} custom-call(bf16[320,512]{1,0:T(8,128)(2,1)} %x_ref.1, f32[2,2048]{1,0:T(2,128)} %pre_ref.1, bf16[2,256,512]{2,1,0:T(8,128)(2,1)} %wv_hbm.1, bf16[2,256,512]{2,1,0:T(8,128)(2,1)} %wg_hbm.1, f32[2,31,512]{2,1,0:T(8,128)} %copy.10.taps_ref, f32[2,512]{1,0:T(2,128)} %ng_ref.1, f32[2,512]{1,0:T(2,128)} %ns_ref.1, ...), custom_call_target="tpu_custom_call" | custom-call | tf_op jit(solution)/shard_map/pallas_call | solution.py:542
  157.3 1.7 %copy.12 = bf16[320,512]{1,0:T(8,128)(2,1)} copy(bf16[320,512]{1,0:T(8,128)(2,1)} %shard_map.91) | data formatting | bytes 655360
where the time goes:
time: 159 us
  Pallas kernels  156 us (98%)
  local copies, waits for them, and re-layouts  3.3 us (2%)
    pallas_call x1, Pallas kernels, kernel_local(): pl.pallas_call(functools.partial(step, nz), out_shape=jax.ShapeDtypeStruc...  156 us
    unnamed x2, local copies, waits for them, and re-layouts  3.3 us

commit v1 on v0

v1 whole, which is shorter than its diff:
```python
import jax
import jax.numpy as jnp
from jax import lax
from jax.experimental import pallas as pl
from jax.experimental.pallas import tpu as pltpu
from jax.sharding import PartitionSpec as P

D = 2048
CONV_WIDTH = 31
LAYERS = 2


EPSILON = 1e-06
LN_EPSILON = 1e-05


def passed_along(block, axis, distance):
    devices = range(lax.axis_size(axis))
    route = [(i - distance, i) for i in devices if i - distance in devices]
    return lax.ppermute(block, axis, route)


def local(tokens, pre_gain, w_value, w_gate, taps, norm_gain, norm_shift, w_out, post_gain):
    stream = tokens
    full_value, full_gate = (
        lax.all_gather(w_value, "sp", axis=1, tiled=True),
        lax.all_gather(w_gate, "sp", axis=1, tiled=True),
    )
    full_out = lax.all_gather(w_out, "sp", axis=2, tiled=True)
    for layer in range(LAYERS):
        whole = lax.all_gather(stream, "tp", axis=1, tiled=True)
        whole_f = whole.astype(jnp.float32)
        normed = (
            whole_f
            * lax.rsqrt(jnp.mean(whole_f * whole_f, -1, keepdims=True) + EPSILON)
            * pre_gain[layer]
        ).astype(jnp.bfloat16)
        value_mat = full_value[layer]
        gate_mat = full_gate[layer]
        out_mat = full_out[layer]
        value_proj = jnp.dot(normed, value_mat, preferred_element_type=jnp.float32)
        gate_proj = jnp.dot(normed, gate_mat, preferred_element_type=jnp.float32)
        glu_act = (value_proj * jax.nn.sigmoid(gate_proj)).astype(jnp.bfloat16)
        rows = glu_act.shape[0]
        fringe = passed_along(glu_act[rows - (CONV_WIDTH - 1) :], "sp", 1)
        padded = jnp.concatenate([fringe, glu_act], 0).astype(jnp.float32)
        conv_out = jnp.zeros(glu_act.shape, jnp.float32)
        for offset in range(CONV_WIDTH):
            conv_out = conv_out + taps[layer, offset] * padded[offset : offset + rows]
        row_sum, row_square = lax.psum(
            (jnp.sum(conv_out, -1, keepdims=True), jnp.sum(conv_out * conv_out, -1, keepdims=True)),
            "tp",
        )
        center = row_sum / D
        spread = jnp.maximum(row_square / D - center * center, 0.0)
        activated = jax.nn.silu(
            (conv_out - center) * lax.rsqrt(spread + LN_EPSILON) * norm_gain[layer]
            + norm_shift[layer]
        ).astype(jnp.bfloat16)
        terms = jnp.dot(activated, out_mat, preferred_element_type=jnp.float32)
        summed = lax.psum_scatter(terms.astype(jnp.bfloat16), "tp", scatter_dimension=1, tiled=True)
        projected = summed.astype(jnp.float32)
        out_square = lax.psum(jnp.sum(projected * projected, -1, keepdims=True), "tp")
        scale = lax.rsqrt(out_square / D + EPSILON)
        stream = (stream.astype(jnp.float32) + projected * scale * post_gain[layer]).astype(
            jnp.bfloat16
        )
    return stream


TILE = 64
PACK = 16
HALO = 32


def step(
    x_ref, pre_ref, wv_hbm, wg_hbm, taps_ref, ng_ref, ns_ref, wo_hbm, post_ref, out_ref,
    weight, other, whole, normed, glu, conv, act, part_out, part_in, x_out, x_in, z_out, z_in,
    total, taps, gain, shift, stat, stat_in, local_sem,
    zs, zr, ys, yr, gs, gr, hs, hr, ss, sr, ps, pr, xs, xr, bs, br,
):
    sp, tp = lax.axis_index("sp"), lax.axis_index("tp")
    rows, cols = x_ref.shape
    layers = pre_ref.shape[0]
    nsp, ntp = 8, 4
    z, y = sp // 2, sp % 2
    zh, zl = z // 2, z % 2
    x, c = tp // 2, tp % 2
    plane = [z, zh * 2 + 1 - zl, (1 - zh) * 2 + zl, (1 - zh) * 2 + 1 - zl]
    partner = plane[1] * 2 + y
    beside, facing = (partner, tp), (z * 2 + 1 - y, tp)
    mate, across, diagonal = (sp, x * 2 + 1 - c), (sp, (1 - x) * 2 + c), (sp, (1 - x) * 2 + 1 - c)
    units = 3 * layers
    both, half = 2 * rows, cols // 2
    mine = pl.ds(pl.multiple_of(zl * half, half), half)
    rest = pl.ds(pl.multiple_of((1 - zl) * half, half), half)
    depth = wv_hbm.shape[1]

    def copy(src, dst, send, recv, to):
        return pltpu.make_async_remote_copy(
            src_ref=src, dst_ref=dst, send_sem=send, recv_sem=recv, device_id=to,
            device_id_type=pl.DeviceIdType.MESH,
        )

    def piece(u, slot):
        return weight.at[u, pl.ds(pl.multiple_of(slot * depth, depth), depth)]

    def along(u, k):
        p = piece(u, sp)
        return copy(
            p if k == 2 else other.at[u], p, zs.at[u, k - 1], zr.at[u, k - 1], (plane[k] * 2 + y, tp)
        )

    def sideways(u, k):
        p = piece(u, plane[k] * 2 + y)
        return copy(p, p, ys.at[u, k], yr.at[u, k], facing)

    def own(u):
        for k in (3, 2, 1):
            along(u, k).start()
        sideways(u, 0).start()

    def relay(u, k):
        p = piece(u, plane[k] * 2 + y)
        copy(p, p, zs.at[u, k - 1], zr.at[u, k - 1], beside).wait_recv()
        sideways(u, k).start()

    def arrive(u):
        for k in range(4):
            p = piece(u, plane[k] * 2 + 1 - y)
            copy(p, p, ys.at[u, k], yr.at[u, k], facing).wait_recv()

    here, there = zl * 4, (1 - zl) * 4
    opposite = (1 - x) * 2 + c

    routes = dict(
        across=(here + tp, across),
        beside=(here + tp, beside),
        mate=(here + tp, mate),
        across_mate=(here + opposite, mate),
        beside_across=(there + tp, across),
        beside_mate=(there + tp, mate),
        both_mate=(there + opposite, mate),
        across_beside=(here + opposite, beside),
    )
    upper, lower = pl.ds(0, rows // 2), pl.ds(rows // 2, rows // 2)
    parts = dict(beside_across=upper, across_beside=lower)

    def gather(l, name):
        k = list(routes).index(name)
        t, to = routes[name]
        b = whole.at[l, t, parts[name]] if name in parts else whole.at[l, t]
        return copy(b, b, gs.at[l, k], gr.at[l, k], to)

    def came(l, k, t, part=pl.ds(0, rows)):
        b = whole.at[l, t, part]
        copy(b, b, gs.at[l, k], gr.at[l, k], mate).wait_recv()

    def gather_start(l):
        for name in ("across", "beside", "mate"):
            gather(l, name).start()

    def gather_turn(l):
        came(l, 1, there + tp)
        gather(l, "beside_across").start()
        gather(l, "beside_mate").start()
        came(l, 0, here + opposite)
        gather(l, "across_beside").start()
        gather(l, "across_mate").start()

    def gather_last(l):
        came(l, 4, there + opposite, upper)
        came(l, 7, there + opposite, lower)
        gather(l, "both_mate").start()

    def gather_wait(l):
        pair_tp, pair_opposite = x * 2 + 1 - c, (1 - x) * 2 + 1 - c
        came(l, 2, here + pair_tp)
        came(l, 3, here + pair_opposite)
        came(l, 5, there + pair_tp)
        came(l, 6, there + pair_opposite)

    def norm(l):
        gather_wait(l)
        tiles = rows // TILE

        @pl.loop(0, 2 * tiles)
        def _(i):
            g, r = i // tiles * 4, pl.ds(pl.multiple_of(i % tiles * TILE, TILE), TILE)
            to = pl.ds(pl.multiple_of(i * TILE, TILE), TILE)
            square = jnp.zeros((TILE, 1), jnp.float32)
            for t in range(ntp):
                v = whole[l, g + t, r, :].astype(jnp.float32)
                square = square + jnp.sum(v * v, -1, keepdims=True)
            scale = lax.rsqrt(square / (cols * ntp) + EPSILON)
            for t in range(ntp):
                v = whole[l, g + t, r, :].astype(jnp.float32)
                at = slice(t * cols, (t + 1) * cols)
                normed[to, at] = (v * scale * pre_ref[l : l + 1, at]).astype(jnp.bfloat16)

    tail, head = pl.ds(rows, HALO), pl.ds(0, HALO)

    def near_halo(l):
        return copy(glu.at[l, 0, tail], glu.at[l, y, head], hs.at[l, 0], hr.at[l, y], facing)

    def even_halo(l):
        return copy(glu.at[l, 1, tail], glu.at[l, 1, head], hs.at[l, 1], hr.at[l, 1], facing)

    def odd_halo(l):
        return copy(
            glu.at[l, 1, tail], glu.at[l, 0, head], hs.at[l, 1], hr.at[l, 0], ((z + 2) * 2, tp)
        )

    def halo_send(l, act_on):
        act_on(near_halo(l))
        pl.when(y == 0)(lambda: act_on(even_halo(l)))
        pl.when((y == 1) & (zh == 0))(lambda: act_on(odd_halo(l)))

    def halo_wait(l):
        def got(q):
            b = glu.at[l, q, head]
            copy(b, b, hs.at[l, q], hr.at[l, q], facing).wait_recv()

        pl.when((y == 1) | (zh == 1))(lambda: got(0))
        got(1)

        @pl.when((y == 0) & (zh == 0))
        def _():
            glu[l, 0, :HALO] = jnp.zeros((HALO, half), jnp.bfloat16)

    def project(l):
        n = normed[...]
        value = jnp.dot(n, weight[3 * l], preferred_element_type=jnp.float32)
        gate = jnp.dot(n, weight[3 * l + 1], preferred_element_type=jnp.float32)
        made = (value * jax.nn.sigmoid(gate)).astype(jnp.bfloat16)
        glu[l, 0, HALO:, :] = made[:rows]
        glu[l, 1, HALO:, :] = made[rows:]
        halo_send(l, lambda h: h.start())

    peers = [mate, across, diagonal, beside]
    peers += [(partner, mate[1]), (partner, across[1]), (partner, diagonal[1])]

    def exchange(e):
        return [
            copy(stat.at[e], stat_in.at[e, j], ss.at[e, j], sr.at[e, j], to)
            for j, to in enumerate(peers[: 3 if e % 2 else 7])
        ]

    def exchanged(e):
        sums = stat[e]
        for j, s in enumerate(exchange(e)):
            s.wait_recv()
            sums = sums + stat_in[e, j]
        return sums

    lane = lax.broadcasted_iota(jnp.int32, (PACK, 128), 1)
    groups = TILE // PACK

    def pick(sums, at):
        found = [
            jnp.sum(jnp.where(lane == at * groups + g, sums, 0.0), -1, keepdims=True)
            for g in range(groups)
        ]
        return jnp.concatenate(found, 0)

    def pack(sums, at, column):
        for g in range(groups):
            sums = jnp.where(lane == at * groups + g, column[g * PACK : (g + 1) * PACK], sums)
        return sums

    tiles = rows // TILE

    def convolve(l):
        first = HALO - (CONV_WIDTH - 1)

        def tile(q, i, sums):
            r = pl.multiple_of(i * TILE, TILE)
            one = jnp.zeros((TILE, 128), jnp.float32)
            two = jnp.zeros((TILE, 128), jnp.float32)
            for j in range(half // 128):
                at = slice(j * 128, (j + 1) * 128)
                window = glu[l, q, pl.ds(r, TILE + HALO), at].astype(jnp.float32)
                acc = jnp.zeros((TILE, 128), jnp.float32)
                for s in range(8):
                    w = window if s == 0 else pltpu.roll(window, TILE + HALO - s, 0)
                    for k in range(CONV_WIDTH):
                        if (first + k) % 8 == s:
                            o = first + k - s
                            acc = acc + taps[l, k : k + 1, at] * w[o : o + TILE]
                conv[q, pl.ds(r, TILE), at] = acc
                one = one + acc
                two = two + acc * acc
            n = q * tiles + i
            sums = pack(sums, 2 * n, jnp.sum(one, -1, keepdims=True))
            return pack(sums, 2 * n + 1, jnp.sum(two, -1, keepdims=True))

        inner = tiles - 1
        sums = lax.fori_loop(
            0, 2 * inner, lambda i, s: tile(i // inner, i % inner + 1, s),
            jnp.zeros((PACK, 128), jnp.float32),
        )
        halo_wait(l)
        stat[2 * l] = lax.fori_loop(0, 2, lambda q, s: tile(q, 0, s), sums)
        for s in exchange(2 * l):
            s.start()

    def activate(l):
        sums = exchanged(2 * l)

        @pl.loop(0, 2 * tiles)
        def _(at):
            q, r = at // tiles, pl.ds(pl.multiple_of(at % tiles * TILE, TILE), TILE)
            center = pick(sums, 2 * at) / (cols * ntp)
            spread = jnp.maximum(pick(sums, 2 * at + 1) / (cols * ntp) - center * center, 0.0)
            v = (conv[q, r, :] - center) * lax.rsqrt(spread + LN_EPSILON)
            v = v * gain[l : l + 1, :] + shift[l : l + 1, :]
            act[q, r, :] = (v * jax.nn.sigmoid(v)).astype(jnp.bfloat16)

    each = wo_hbm.shape[2]
    per = cols // each
    quads = dict(D=(1 - zl, 1 - x), A=(zl, 1 - x), B=(1 - zl, x), O=(zl, x))
    names = list(quads)

    def term(l, quad, h, core):
        q, column = quads[quad]
        slot = (column * 2 + core) * per + h
        w = weight[3 * l + 2, pl.ds(pl.multiple_of(slot * depth, depth), depth), :]
        return jnp.dot(act[q], w, preferred_element_type=jnp.float32).astype(jnp.bfloat16)

    def pair(l, quad, h):
        i = names.index(quad) * per + h
        return copy(part_out.at[l, i], part_in.at[l, i], ps.at[l, i], pr.at[l, i], mate)

    def over(l, i):
        return copy(x_out.at[l, i], x_in.at[l, i], xs.at[l, i], xr.at[l, i], across)

    def along_pair(l, i):
        return copy(z_out.at[l, i], z_in.at[l, i], bs.at[l, i], br.at[l, i], beside)

    def give(l, quad, h):
        part_out[l, names.index(quad) * per + h] = term(l, quad, h, 1 - c)
        pair(l, quad, h).start()

    def joined(l, quad, h):
        kept = term(l, quad, h, c).astype(jnp.float32)
        pair(l, quad, h).wait_recv()
        return kept + part_in[l, names.index(quad) * per + h].astype(jnp.float32)

    def pass_x(l, i, v):
        x_out[l, i] = v.astype(jnp.bfloat16)
        over(l, i).start()

    def pass_z(l, i, v):
        z_out[l, i] = v.astype(jnp.bfloat16)
        along_pair(l, i).start()

    def reduce(l, between):
        give(l, "D", 0)
        give(l, "D", 1)
        give(l, "A", 0)
        give(l, "B", 1)
        pass_x(l, 0, joined(l, "D", 0))
        pass_z(l, 0, joined(l, "D", 1))
        give(l, "A", 1)
        give(l, "B", 0)
        pass_x(l, 1, joined(l, "A", 0))
        pass_z(l, 1, joined(l, "B", 1))
        give(l, "O", 0)
        give(l, "O", 1)
        for h in range(per):
            total[:, h * each : (h + 1) * each] = joined(l, "O", h)
        from_beside = joined(l, "A", 1)
        along_pair(l, 0).wait_recv()
        pass_x(l, 2, from_beside + z_in[l, 0].astype(jnp.float32))
        from_across = joined(l, "B", 0)
        over(l, 0).wait_recv()
        pass_z(l, 2, from_across + x_in[l, 0].astype(jnp.float32))
        between()

    def finish(l):
        over(l, 1).wait_recv()
        along_pair(l, 1).wait_recv()
        over(l, 2).wait_recv()
        along_pair(l, 2).wait_recv()

        def tile(i, sums):
            r = pl.ds(pl.multiple_of(i * TILE, TILE), TILE)
            square = jnp.zeros((TILE, 1), jnp.float32)
            for h in range(per):
                at = slice(h * each, (h + 1) * each)
                p = total[r, at] + x_in[l, 1 + h, r, :].astype(jnp.float32)
                p = p + z_in[l, 2 - h, r, :].astype(jnp.float32)
                p = p.astype(jnp.bfloat16).astype(jnp.float32)
                total[r, at] = p
                square = square + jnp.sum(p * p, -1, keepdims=True)
            return pack(sums, i, square)

        e = 2 * l + 1
        stat[e] = lax.fori_loop(0, tiles, tile, jnp.zeros((PACK, 128), jnp.float32))
        for s in exchange(e):
            s.start()
        sums = exchanged(e)

        @pl.loop(0, tiles)
        def _(i):
            r = pl.ds(pl.multiple_of(i * TILE, TILE), TILE)
            scale = lax.rsqrt(pick(sums, i) / (cols * ntp) + EPSILON)
            old = whole[l, here + tp, r, :].astype(jnp.float32)
            new = (old + total[r, :] * scale * post_ref[l : l + 1, :]).astype(jnp.bfloat16)
            if l + 1 < layers:
                whole[l + 1, here + tp, r, :] = new
            else:
                out_ref[r, :] = new

    held = [pltpu.make_async_copy(x_ref, whole.at[0, here + tp], local_sem.at[2 * units])]
    for u in range(units):
        l, kind = divmod(u, 3)
        ref = (wv_hbm, wg_hbm, wo_hbm)[kind]
        for i, (part, to) in enumerate(((mine, piece(u, sp)), (rest, other.at[u]))):
            src = ref.at[l, part] if kind == 2 else ref.at[l, :, part]
            held.append(pltpu.make_async_copy(src, to, local_sem.at[2 * u + i]))
    for h in held:
        h.start()
    for l in range(layers):
        taps[l] = taps_ref[l, :, mine]
        gain[l : l + 1] = ng_ref[l : l + 1, mine]
        shift[l : l + 1] = ns_ref[l : l + 1, mine]
    barrier = pltpu.get_barrier_semaphore()
    for i in range(1, nsp):
        pl.semaphore_signal(
            barrier, inc=1, device_id=(lax.rem(sp + i, nsp), tp),
            device_id_type=pl.DeviceIdType.MESH,
        )
    for i in range(1, ntp):
        for at in (sp, partner):
            pl.semaphore_signal(
                barrier, inc=1, device_id=(at, lax.rem(tp + i, ntp)),
                device_id_type=pl.DeviceIdType.MESH,
            )
    pl.semaphore_wait(barrier, nsp - 1 + 2 * (ntp - 1))
    for h in held:
        h.wait()

    far = range(1, 4)
    gather_start(0)
    own(0)
    own(1)
    gather_turn(0)
    own(2)
    for k in far:
        relay(0, k)
    gather_last(0)
    norm(0)
    for k in far:
        relay(1, k)
    arrive(0)
    arrive(1)
    project(0)
    relay(2, 1)
    convolve(0)
    relay(2, 2)
    relay(2, 3)
    activate(0)
    arrive(2)
    reduce(0, lambda: (own(3), own(4)))
    finish(0)
    gather_start(1)
    own(5)
    for k in far:
        relay(3, k)
    gather_turn(1)
    for k in far:
        relay(4, k)
    gather_last(1)
    norm(1)
    arrive(3)
    arrive(4)
    project(1)
    relay(5, 1)
    convolve(1)
    relay(5, 2)
    relay(5, 3)
    activate(1)
    arrive(5)
    reduce(1, lambda: None)
    finish(1)

    sent = [along(u, k) for u in range(units) for k in far]
    sent += [sideways(u, k) for u in range(units) for k in range(4)]
    for l in range(layers):
        sent += [gather(l, name) for name in routes]
        sent += [*exchange(2 * l), *exchange(2 * l + 1)]
        sent += [over(l, i) for i in range(3)] + [along_pair(l, i) for i in range(3)]
        sent += [pair(l, quad, h) for quad in names for h in range(per)]
        halo_send(l, lambda h: h.wait_send())
    for s in sent:
        s.wait_send()


def kernel_local(*args):
    tokens, pre_gain, w_value, _, _, _, _, w_out, _ = args
    rows, cols = tokens.shape
    layers, depth = w_value.shape[:2]
    each = w_out.shape[2]
    half, units = cols // 2, 3 * layers
    if rows % TILE or 2 * 2 * rows > PACK * 128 or not depth == half == each:
        return local(*args)
    vmem, hbm = pl.BlockSpec(memory_space=pltpu.VMEM), pl.BlockSpec(memory_space=pl.ANY)
    bf16, f32, dma = jnp.bfloat16, jnp.float32, pltpu.SemaphoreType.DMA
    return pl.pallas_call(
        step,
        out_shape=jax.ShapeDtypeStruct((rows, cols), bf16),
        in_specs=[hbm, vmem, hbm, hbm, vmem, vmem, vmem, hbm, vmem],
        out_specs=vmem,
        scratch_shapes=[
            pltpu.VMEM((units, 8 * depth, half), bf16),
            pltpu.VMEM((units, depth, half), bf16),
            pltpu.VMEM((layers, 8, rows, cols), bf16),
            pltpu.VMEM((2 * rows, 4 * cols), bf16),
            pltpu.VMEM((layers, 2, HALO + rows, half), bf16),
            pltpu.VMEM((2, rows, half), f32),
            pltpu.VMEM((2, rows, half), bf16),
            pltpu.VMEM((layers, 8, rows, each), bf16),
            pltpu.VMEM((layers, 8, rows, each), bf16),
            pltpu.VMEM((layers, 3, rows, each), bf16),
            pltpu.VMEM((layers, 3, rows, each), bf16),
            pltpu.VMEM((layers, 3, rows, each), bf16),
            pltpu.VMEM((layers, 3, rows, each), bf16),
            pltpu.VMEM((rows, cols), f32),
            pltpu.VMEM((layers, CONV_WIDTH, half), f32),
            pltpu.VMEM((layers, half), f32),
            pltpu.VMEM((layers, half), f32),
            pltpu.VMEM((2 * layers, PACK, 128), f32),
            pltpu.VMEM((2 * layers, 7, PACK, 128), f32),
            dma((2 * units + 1,)),
            dma((units, 3)), dma((units, 3)),
            dma((units, 4)), dma((units, 4)),
            dma((layers, 8)), dma((layers, 8)),
            dma((layers, 2)), dma((layers, 2)),
            dma((2 * layers, 7)), dma((2 * layers, 7)),
            dma((layers, 8)), dma((layers, 8)),
            dma((layers, 3)), dma((layers, 3)),
            dma((layers, 3)), dma((layers, 3)),
        ],
        compiler_params=pltpu.CompilerParams(
            collective_id=0, has_side_effects=True, vmem_limit_bytes=56 * 1024 * 1024
        ),
    )(*args)


def solution(mesh):
    nsp, ntp = mesh.shape["sp"], mesh.shape["tp"]
    body = kernel_local if nsp == 8 and ntp == 4 else local
    placed = (
        P("sp", "tp"),
        P(),
        P(None, "sp", "tp"),
        P(None, "sp", "tp"),
        P(None, None, "tp"),
        P(None, "tp"),
        P(None, "tp"),
        P(None, "tp", "sp"),
        P(None, "tp"),
    )
    return jax.shard_map(
        body, mesh=mesh, in_specs=placed, out_specs=P("sp", "tp"), check_vma=False
    )
```

time: 159 us -> 158 us (level)
  no operation moved by 1% of the time
where the time goes in v1:
time: 158 us
  Pallas kernels  155 us (98%)
  local copies, waits for them, and re-layouts  3.3 us (2%)
    pallas_call x1, Pallas kernels, kernel_local(): pl.pallas_call(step, out_shape=jax.ShapeDtypeStruct((rows, cols), bf16),...  155 us
    unnamed x2, local copies, waits for them, and re-layouts  3.3 us

profile of v1, /device:TPU:0, one launch (start us, length us, event | category | flops | bytes accessed | tf_op | source)
XLA Modules:
  0.0 158.1 jit_solution(15773576076797707104)
XLA Ops:
  0.0 1.6 %copy.10.taps_ref = f32[2,31,512]{2,1,0:T(8,128)} copy(f32[2,31,512]{2,0,1:T(2,128)} %param.13) | data formatting | bytes 253952 | tf_op args[4]
  1.6 154.8 %shard_map.91 = bf16[320,512]{1,0:T(8,128)(2,1)} custom-call(bf16[320,512]{1,0:T(8,128)(2,1)} %x_ref.1, f32[2,2048]{1,0:T(2,128)} %pre_ref.1, bf16[2,256,512]{2,1,0:T(8,128)(2,1)} %wv_hbm.1, bf16[2,256,512]{2,1,0:T(8,128)(2,1)} %wg_hbm.1, f32[2,31,512]{2,1,0:T(8,128)} %copy.10.taps_ref, f32[2,512]{1,0:T(2,128)} %ng_ref.1, f32[2,512]{1,0:T(2,128)} %ns_ref.1, ...), custom_call_target="tpu_custom_call" | custom-call | tf_op jit(solution)/shard_map/pallas_call | solution.py:510
  156.4 1.7 %copy.12 = bf16[320,512]{1,0:T(8,128)(2,1)} copy(bf16[320,512]{1,0:T(8,128)(2,1)} %shard_map.91) | data formatting | bytes 655360

commit v2 on v1

--- a/solution.py
+++ b/solution.py
@@ -71,13 +71,15 @@
 TILE = 64
 PACK = 16
 HALO = 32
+DIAGONAL_FIRST_X = ((True, True), (True, False))
+DIAGONAL_X = (True, True)
 
 
 def step(
     x_ref, pre_ref, wv_hbm, wg_hbm, taps_ref, ng_ref, ns_ref, wo_hbm, post_ref, out_ref,
-    weight, other, whole, normed, glu, conv, act, part_out, part_in, x_out, x_in, z_out, z_in,
-    total, taps, gain, shift, stat, stat_in, local_sem,
-    zs, zr, ys, yr, gs, gr, hs, hr, ss, sr, ps, pr, xs, xr, bs, br,
+    weight, other, whole, shared, normed, glu, conv, act, part_out, part_in, x_out, x_in, z_out, z_in,
+    total, taps, gain, shift, stat, stat_in, post_all, local_sem,
+    zs, zr, ys, yr, gs, gr, fs, fr, hs, hr, ss, sr, ps, pr, xs, xr, bs, br, qs, qr,
 ):
     sp, tp = lax.axis_index("sp"), lax.axis_index("tp")
     rows, cols = x_ref.shape
@@ -116,9 +118,8 @@
         return copy(p, p, ys.at[u, k], yr.at[u, k], facing)
 
     def own(u):
-        for k in (3, 2, 1):
+        for k in (1, 2, 3):
             along(u, k).start()
-        sideways(u, 0).start()
 
     def relay(u, k):
         p = piece(u, plane[k] * 2 + y)
@@ -133,56 +134,67 @@
     here, there = zl * 4, (1 - zl) * 4
     opposite = (1 - x) * 2 + c
 
+    upper, lower = pl.ds(0, rows // 2), pl.ds(rows // 2, rows // 2)
+    full = pl.ds(0, rows)
     routes = dict(
-        across=(here + tp, across),
-        beside=(here + tp, beside),
-        mate=(here + tp, mate),
-        across_mate=(here + opposite, mate),
-        beside_across=(there + tp, across),
-        beside_mate=(there + tp, mate),
-        both_mate=(there + opposite, mate),
-        across_beside=(here + opposite, beside),
+        across=(here + tp, full, across),
+        beside_upper=(here + tp, upper, beside),
+        beside_lower=(here + tp, lower, beside),
+        mate=(here + tp, full, mate),
+        diagonal_upper=(there + tp, upper, across),
+        diagonal_lower=(there + tp, lower, across),
+        across_mate=(here + opposite, full, mate),
+        beside_mate=(there + tp, full, mate),
+        both_mate_upper=(there + opposite, upper, mate),
+        both_mate_lower=(there + opposite, lower, mate),
     )
-    upper, lower = pl.ds(0, rows // 2), pl.ds(rows // 2, rows // 2)
-    parts = dict(beside_across=upper, across_beside=lower)
-
-    def gather(l, name):
+
+    def gather(name):
         k = list(routes).index(name)
-        t, to = routes[name]
-        b = whole.at[l, t, parts[name]] if name in parts else whole.at[l, t]
-        return copy(b, b, gs.at[l, k], gr.at[l, k], to)
-
-    def came(l, k, t, part=pl.ds(0, rows)):
-        b = whole.at[l, t, part]
-        copy(b, b, gs.at[l, k], gr.at[l, k], mate).wait_recv()
-
-    def gather_start(l):
-        for name in ("across", "beside", "mate"):
-            gather(l, name).start()
-
-    def gather_turn(l):
-        came(l, 1, there + tp)
-        gather(l, "beside_across").start()
-        gather(l, "beside_mate").start()
-        came(l, 0, here + opposite)
-        gather(l, "across_beside").start()
-        gather(l, "across_mate").start()
-
-    def gather_last(l):
-        came(l, 4, there + opposite, upper)
-        came(l, 7, there + opposite, lower)
-        gather(l, "both_mate").start()
-
-    def gather_wait(l):
-        pair_tp, pair_opposite = x * 2 + 1 - c, (1 - x) * 2 + 1 - c
-        came(l, 2, here + pair_tp)
-        came(l, 3, here + pair_opposite)
-        came(l, 5, there + pair_tp)
-        came(l, 6, there + pair_opposite)
-
-    def norm(l):
-        gather_wait(l)
-        tiles = rows // TILE
+        t, part, to = routes[name]
+        b = whole.at[0, t, part]
+        return copy(b, b, gs.at[k], gr.at[k], to)
+
+    def came(name, t):
+        k = list(routes).index(name)
+        b = whole.at[0, t, routes[name][1]]
+        copy(b, b, gs.at[k], gr.at[k], mate).wait_recv()
+
+    def gather_start():
+        for name in ("across", "beside_upper", "beside_lower", "mate"):
+            gather(name).start()
+
+    def gather_upper():
+        came("beside_upper", there + tp)
+        gather("diagonal_upper").start()
+
+    def gather_lower():
+        came("beside_lower", there + tp)
+        gather("diagonal_lower").start()
+        gather("beside_mate").start()
+
+    def gather_across():
+        came("across", here + opposite)
+        gather("across_mate").start()
+
+    def gather_last():
+        came("diagonal_upper", there + opposite)
+        gather("both_mate_upper").start()
+        came("diagonal_lower", there + opposite)
+        gather("both_mate_lower").start()
+
+    pair_tp, pair_opposite = x * 2 + 1 - c, (1 - x) * 2 + 1 - c
+    tiles = rows // TILE
+
+    def row_scale(square):
+        return lax.rsqrt(square / (cols * ntp) + EPSILON)
+
+    def norm():
+        came("mate", here + pair_tp)
+        came("across_mate", here + pair_opposite)
+        came("beside_mate", there + pair_tp)
+        came("both_mate_upper", there + pair_opposite)
+        came("both_mate_lower", there + pair_opposite)
 
         @pl.loop(0, 2 * tiles)
         def _(i):
@@ -190,13 +202,93 @@
             to = pl.ds(pl.multiple_of(i * TILE, TILE), TILE)
             square = jnp.zeros((TILE, 1), jnp.float32)
             for t in range(ntp):
-                v = whole[l, g + t, r, :].astype(jnp.float32)
+                v = whole[0, g + t, r, :].astype(jnp.float32)
                 square = square + jnp.sum(v * v, -1, keepdims=True)
-            scale = lax.rsqrt(square / (cols * ntp) + EPSILON)
+            scale = row_scale(square)
             for t in range(ntp):
-                v = whole[l, g + t, r, :].astype(jnp.float32)
+                v = whole[0, g + t, r, :].astype(jnp.float32)
                 at = slice(t * cols, (t + 1) * cols)
-                normed[to, at] = (v * scale * pre_ref[l : l + 1, at]).astype(jnp.bfloat16)
+                normed[to, at] = (v * scale * pre_ref[0:1, at]).astype(jnp.bfloat16)
+
+    hand = [
+        dict(
+            across=(here + tp, across, here + opposite),
+            beside=(here + tp, beside, there + tp),
+            mate=(here + tp, mate, here + pair_tp),
+            diagonal=(
+                (there + tp if DIAGONAL_X[h] else here + opposite),
+                (across if DIAGONAL_X[h] else beside),
+                there + opposite,
+            ),
+            across_mate=(here + opposite, mate, here + pair_opposite),
+            beside_mate=(there + tp, mate, there + pair_tp),
+            both_mate=(there + opposite, mate, there + pair_opposite),
+        )
+        for h in range(2)
+    ]
+
+    def share(l, name, h):
+        k = list(hand[h]).index(name) * 2 + h
+        t, to, _ = hand[h][name]
+        b = shared.at[l, t, h]
+        return copy(b, b, fs.at[l, k], fr.at[l, k], to)
+
+    def shared_wait(l, name, h):
+        k = list(hand[h]).index(name) * 2 + h
+        b = shared.at[l, hand[h][name][2], h]
+        copy(b, b, fs.at[l, k], fr.at[l, k], mate).wait_recv()
+
+    def share_start(l, h):
+        for name in ("across", "beside", "mate"):
+            share(l, name, h).start()
+
+    def share_turn(l, name, h):
+        shared_wait(l, name, h)
+        if (name == "beside") == DIAGONAL_X[h]:
+            share(l, "diagonal", h).start()
+        share(l, name + "_mate", h).start()
+
+    def share_last(l, h):
+        shared_wait(l, "diagonal", h)
+        share(l, "both_mate", h).start()
+
+    def post_copy(j):
+        return copy(post_ref, post_all.at[tp], qs.at[j], qr.at[j], (mate, across, diagonal)[j])
+
+    def post_wait(j):
+        t = (pair_tp, opposite, pair_opposite)[j]
+        copy(post_ref, post_all.at[t], qs.at[j], qr.at[j], mate).wait_recv()
+
+    def norm_next(l):
+        for h in range(per):
+            for name in ("mate", "across_mate", "beside_mate", "both_mate"):
+                shared_wait(l, name, h)
+
+        @pl.loop(0, 2 * tiles)
+        def _(i):
+            g, r = i // tiles * 4, pl.ds(pl.multiple_of(i % tiles * TILE, TILE), TILE)
+            to = pl.ds(pl.multiple_of(i * TILE, TILE), TILE)
+            square = jnp.zeros((TILE, 1), jnp.float32)
+            for t in range(ntp):
+                for h in range(per):
+                    v = shared[l, g + t, h, r, :].astype(jnp.float32)
+                    square = square + jnp.sum(v * v, -1, keepdims=True)
+            scale = row_scale(square)
+            square = jnp.zeros((TILE, 1), jnp.float32)
+            for t in range(ntp):
+                for h in range(per):
+                    at = slice(h * each, (h + 1) * each)
+                    v = shared[l, g + t, h, r, :].astype(jnp.float32)
+                    old = whole[l, g + t, r, at].astype(jnp.float32)
+                    new = (old + v * scale * post_all[t, l : l + 1, at]).astype(jnp.bfloat16)
+                    whole[l + 1, g + t, r, at] = new
+                    v = new.astype(jnp.float32)
+                    square = square + jnp.sum(v * v, -1, keepdims=True)
+            scale = row_scale(square)
+            for t in range(ntp):
+                v = whole[l + 1, g + t, r, :].astype(jnp.float32)
+                at = slice(t * cols, (t + 1) * cols)
+                normed[to, at] = (v * scale * pre_ref[l + 1 : l + 2, at]).astype(jnp.bfloat16)
 
     tail, head = pl.ds(rows, HALO), pl.ds(0, HALO)
 
@@ -267,8 +359,6 @@
         for g in range(groups):
             sums = jnp.where(lane == at * groups + g, column[g * PACK : (g + 1) * PACK], sums)
         return sums
-
-    tiles = rows // TILE
 
     def convolve(l):
         first = HALO - (CONV_WIDTH - 1)
@@ -304,18 +394,24 @@
         for s in exchange(2 * l):
             s.start()
 
-    def activate(l):
-        sums = exchanged(2 * l)
-
-        @pl.loop(0, 2 * tiles)
-        def _(at):
-            q, r = at // tiles, pl.ds(pl.multiple_of(at % tiles * TILE, TILE), TILE)
+    def activate(l, q):
+        sums = stat[2 * l]
+        for j in range(7):
+            sums = sums + stat_in[2 * l, j]
+
+        @pl.loop(0, tiles)
+        def _(i):
+            at, r = q * tiles + i, pl.ds(pl.multiple_of(i * TILE, TILE), TILE)
             center = pick(sums, 2 * at) / (cols * ntp)
             spread = jnp.maximum(pick(sums, 2 * at + 1) / (cols * ntp) - center * center, 0.0)
             v = (conv[q, r, :] - center) * lax.rsqrt(spread + LN_EPSILON)
             v = v * gain[l : l + 1, :] + shift[l : l + 1, :]
             act[q, r, :] = (v * jax.nn.sigmoid(v)).astype(jnp.bfloat16)
 
+    def moments(l):
+        for s in exchange(2 * l):
+            s.wait_recv()
+
     each = wo_hbm.shape[2]
     per = cols // each
     quads = dict(D=(1 - zl, 1 - x), A=(zl, 1 - x), B=(1 - zl, x), O=(zl, x))
@@ -354,44 +450,56 @@
         z_out[l, i] = v.astype(jnp.bfloat16)
         along_pair(l, i).start()
 
-    def reduce(l, between):
-        give(l, "D", 0)
-        give(l, "D", 1)
-        give(l, "A", 0)
-        give(l, "B", 1)
-        pass_x(l, 0, joined(l, "D", 0))
-        pass_z(l, 0, joined(l, "D", 1))
-        give(l, "A", 1)
-        give(l, "B", 0)
-        pass_x(l, 1, joined(l, "A", 0))
-        pass_z(l, 1, joined(l, "B", 1))
-        give(l, "O", 0)
-        give(l, "O", 1)
+    def move_on(l, quad, h):
+        v = joined(l, quad, h)
+        if quad == "O":
+            total[:, h * each : (h + 1) * each] = v
+        elif quad == "A":
+            if not DIAGONAL_FIRST_X[l][h]:
+                along_pair(l, h).wait_recv()
+                v = v + z_in[l, h].astype(jnp.float32)
+            pass_x(l, 2 + h, v)
+        elif quad == "B":
+            if DIAGONAL_FIRST_X[l][h]:
+                over(l, h).wait_recv()
+                v = v + x_in[l, h].astype(jnp.float32)
+            pass_z(l, 2 + h, v)
+        elif DIAGONAL_FIRST_X[l][h]:
+            pass_x(l, h, v)
+        else:
+            pass_z(l, h, v)
+
+    def steps(l, names):
+        for name in names.split():
+            (give if name[0] == "g" else move_on)(l, name[1], int(name[2]))
+
+    def projected(l, h, r):
+        at = slice(h * each, (h + 1) * each)
+        p = total[r, at] + x_in[l, 2 + h, r, :].astype(jnp.float32)
+        return (p + z_in[l, 2 + h, r, :].astype(jnp.float32)).astype(jnp.bfloat16)
+
+    def settle(l, h):
+        over(l, 2 + h).wait_recv()
+        along_pair(l, 2 + h).wait_recv()
+
+        @pl.loop(0, tiles)
+        def _(i):
+            r = pl.ds(pl.multiple_of(i * TILE, TILE), TILE)
+            shared[l, here + tp, h, r, :] = projected(l, h, r)
+
+        share_start(l, h)
+
+    def finish(l):
         for h in range(per):
-            total[:, h * each : (h + 1) * each] = joined(l, "O", h)
-        from_beside = joined(l, "A", 1)
-        along_pair(l, 0).wait_recv()
-        pass_x(l, 2, from_beside + z_in[l, 0].astype(jnp.float32))
-        from_across = joined(l, "B", 0)
-        over(l, 0).wait_recv()
-        pass_z(l, 2, from_across + x_in[l, 0].astype(jnp.float32))
-        between()
-
-    def finish(l):
-        over(l, 1).wait_recv()
-        along_pair(l, 1).wait_recv()
-        over(l, 2).wait_recv()
-        along_pair(l, 2).wait_recv()
+            over(l, 2 + h).wait_recv()
+            along_pair(l, 2 + h).wait_recv()
 
         def tile(i, sums):
             r = pl.ds(pl.multiple_of(i * TILE, TILE), TILE)
             square = jnp.zeros((TILE, 1), jnp.float32)
             for h in range(per):
-                at = slice(h * each, (h + 1) * each)
-                p = total[r, at] + x_in[l, 1 + h, r, :].astype(jnp.float32)
-                p = p + z_in[l, 2 - h, r, :].astype(jnp.float32)
-                p = p.astype(jnp.bfloat16).astype(jnp.float32)
-                total[r, at] = p
+                p = projected(l, h, r).astype(jnp.float32)
+                total[r, h * each : (h + 1) * each] = p
                 square = square + jnp.sum(p * p, -1, keepdims=True)
             return pack(sums, i, square)
 
@@ -404,13 +512,9 @@
         @pl.loop(0, tiles)
         def _(i):
             r = pl.ds(pl.multiple_of(i * TILE, TILE), TILE)
-            scale = lax.rsqrt(pick(sums, i) / (cols * ntp) + EPSILON)
             old = whole[l, here + tp, r, :].astype(jnp.float32)
-            new = (old + total[r, :] * scale * post_ref[l : l + 1, :]).astype(jnp.bfloat16)
-            if l + 1 < layers:
-                whole[l + 1, here + tp, r, :] = new
-            else:
-                out_ref[r, :] = new
+            new = old + total[r, :] * row_scale(pick(sums, i)) * post_ref[l : l + 1, :]
+            out_ref[r, :] = new.astype(jnp.bfloat16)
 
     held = [pltpu.make_async_copy(x_ref, whole.at[0, here + tp], local_sem.at[2 * units])]
     for u in range(units):
@@ -421,8 +525,9 @@
             held.append(pltpu.make_async_copy(src, to, local_sem.at[2 * u + i]))
     for h in held:
         h.start()
+    post_all[tp] = post_ref[...]
     for l in range(layers):
-        taps[l] = taps_ref[l, :, mine]
+        taps[l] = taps_ref[:, l, mine]
         gain[l : l + 1] = ng_ref[l : l + 1, mine]
         shift[l : l + 1] = ns_ref[l : l + 1, mine]
     barrier = pltpu.get_barrier_semaphore()
@@ -442,63 +547,93 @@
         h.wait()
 
     far = range(1, 4)
-    gather_start(0)
     own(0)
+    sideways(0, 0).start()
+    gather_start()
+    for j in range(3):
+        post_copy(j).start()
     own(1)
-    gather_turn(0)
-    own(2)
+    sideways(1, 0).start()
     for k in far:
         relay(0, k)
-    gather_last(0)
-    norm(0)
-    for k in far:
-        relay(1, k)
+    gather_upper()
+    relay(1, 2)
+    gather_lower()
+    relay(1, 3)
+    gather_across()
+    own(2)
+    relay(1, 1)
+    sideways(2, 0).start()
+    gather_last()
+    norm()
     arrive(0)
     arrive(1)
     project(0)
     relay(2, 1)
+    relay(2, 2)
     convolve(0)
-    relay(2, 2)
+    own(3)
+    own(4)
     relay(2, 3)
-    activate(0)
+    moments(0)
+    activate(0, 1 - zl)
     arrive(2)
-    reduce(0, lambda: (own(3), own(4)))
-    finish(0)
-    gather_start(1)
-    own(5)
+    steps(0, "gD0 gD1 mD0 mD1")
+    activate(0, zl)
+    steps(0, "gA0 gA1 gB0 gB1 mA0 mA1 gO0 gO1 mB0 mB1 mO0 mO1")
+    sideways(3, 0).start()
     for k in far:
         relay(3, k)
-    gather_turn(1)
+    settle(0, 0)
+    settle(0, 1)
+    own(5)
+    sideways(4, 0).start()
+    share_turn(0, "beside", 0)
     for k in far:
         relay(4, k)
-    gather_last(1)
-    norm(1)
+    share_turn(0, "beside", 1)
+    share_turn(0, "across", 0)
+    share_turn(0, "across", 1)
+    sideways(5, 0).start()
+    share_last(0, 0)
+    share_last(0, 1)
+    for j in range(3):
+        post_wait(j)
+    norm_next(0)
     arrive(3)
     arrive(4)
     project(1)
-    relay(5, 1)
+    for k in far:
+        relay(5, k)
     convolve(1)
-    relay(5, 2)
-    relay(5, 3)
-    activate(1)
+    moments(1)
+    activate(1, 1 - zl)
     arrive(5)
-    reduce(1, lambda: None)
+    steps(1, "gD0 gD1 mD0 mD1")
+    activate(1, zl)
+    steps(1, "gA0 gB1 gA1 gB0 mA0 mB1 gO0 gO1 mO0 mO1 mA1 mB0")
     finish(1)
 
     sent = [along(u, k) for u in range(units) for k in far]
     sent += [sideways(u, k) for u in range(units) for k in range(4)]
+    sent += [gather(name) for name in routes] + [post_copy(j) for j in range(3)]
     for l in range(layers):
-        sent += [gather(l, name) for name in routes]
-        sent += [*exchange(2 * l), *exchange(2 * l + 1)]
-        sent += [over(l, i) for i in range(3)] + [along_pair(l, i) for i in range(3)]
-        sent += [pair(l, quad, h) for quad in names for h in range(per)]
+        sent += exchange(2 * l)
+        if l + 1 < layers:
+            sent += [share(l, name, h) for h in range(per) for name in hand[h]]
+        else:
+            sent += exchange(2 * l + 1)
+        for h in range(per):
+            sent += [over(l, 2 + h), along_pair(l, 2 + h)]
+            sent.append(over(l, h) if DIAGONAL_FIRST_X[l][h] else along_pair(l, h))
+            sent += [pair(l, quad, h) for quad in names]
         halo_send(l, lambda h: h.wait_send())
     for s in sent:
         s.wait_send()
 
 
 def kernel_local(*args):
-    tokens, pre_gain, w_value, _, _, _, _, w_out, _ = args
+    tokens, pre_gain, w_value, w_gate, all_taps, norm_gain, norm_shift, w_out, post_gain = args
     rows, cols = tokens.shape
     layers, depth = w_value.shape[:2]
     each = w_out.shape[2]
@@ -516,36 +651,43 @@
             pltpu.VMEM((units, 8 * depth, half), bf16),
             pltpu.VMEM((units, depth, half), bf16),
             pltpu.VMEM((layers, 8, rows, cols), bf16),
+            pltpu.VMEM((layers - 1, 8, 2, rows, each), bf16),
             pltpu.VMEM((2 * rows, 4 * cols), bf16),
             pltpu.VMEM((layers, 2, HALO + rows, half), bf16),
             pltpu.VMEM((2, rows, half), f32),
             pltpu.VMEM((2, rows, half), bf16),
             pltpu.VMEM((layers, 8, rows, each), bf16),
             pltpu.VMEM((layers, 8, rows, each), bf16),
-            pltpu.VMEM((layers, 3, rows, each), bf16),
-            pltpu.VMEM((layers, 3, rows, each), bf16),
-            pltpu.VMEM((layers, 3, rows, each), bf16),
-            pltpu.VMEM((layers, 3, rows, each), bf16),
+            pltpu.VMEM((layers, 4, rows, each), bf16),
+            pltpu.VMEM((layers, 4, rows, each), bf16),
+            pltpu.VMEM((layers, 4, rows, each), bf16),
+            pltpu.VMEM((layers, 4, rows, each), bf16),
             pltpu.VMEM((rows, cols), f32),
             pltpu.VMEM((layers, CONV_WIDTH, half), f32),
             pltpu.VMEM((layers, half), f32),
             pltpu.VMEM((layers, half), f32),
             pltpu.VMEM((2 * layers, PACK, 128), f32),
             pltpu.VMEM((2 * layers, 7, PACK, 128), f32),
+            pltpu.VMEM((4, layers, cols), f32),
             dma((2 * units + 1,)),
             dma((units, 3)), dma((units, 3)),
             dma((units, 4)), dma((units, 4)),
-            dma((layers, 8)), dma((layers, 8)),
+            dma((10,)), dma((10,)),
+            dma((layers - 1, 14)), dma((layers - 1, 14)),
             dma((layers, 2)), dma((layers, 2)),
             dma((2 * layers, 7)), dma((2 * layers, 7)),
             dma((layers, 8)), dma((layers, 8)),
-            dma((layers, 3)), dma((layers, 3)),
-            dma((layers, 3)), dma((layers, 3)),
+            dma((layers, 4)), dma((layers, 4)),
+            dma((layers, 4)), dma((layers, 4)),
+            dma((3,)), dma((3,)),
         ],
         compiler_params=pltpu.CompilerParams(
             collective_id=0, has_side_effects=True, vmem_limit_bytes=56 * 1024 * 1024
         ),
-    )(*args)
+    )(
+        tokens, pre_gain, w_value, w_gate, jnp.swapaxes(all_taps, 0, 1), norm_gain, norm_shift, w_out,
+        post_gain,
+    )
 
 
 def solution(mesh):

time: 158 us -> 126 us (0.80)
  Pallas kernels: 155 us -> 123 us
    pallas_call x1, Pallas kernels: 155 us -> 123 us  [kernel_local(): pl.pallas_call(step, out_shape=jax.ShapeDtypeStruct((rows, cols), bf16),...]
    unnamed x2 -> x1, local copies, waits for them, and re-layouts: 3.3 us -> 1.72 us
where the time goes in v2:
time: 126 us; the launch traced here: 125 us
  Pallas kernels  123 us (98%)
  local copies, waits for them, and re-layouts  1.72 us (1%)
    pallas_call x1, Pallas kernels, kernel_local(): pl.pallas_call(step, out_shape=jax.ShapeDtypeStruct((rows, cols), bf16),...  123 us

profile of v2, /device:TPU:0, one launch (start us, length us, event | category | flops | bytes accessed | tf_op | source)
XLA Modules:
  0.0 124.8 jit_solution(17595300564856532979)
XLA Ops:
  0.0 123.1 %shard_map.91 = bf16[320,512]{1,0:T(8,128)(2,1)} custom-call(bf16[320,512]{1,0:T(8,128)(2,1)} %x_ref.1, f32[2,2048]{1,0:T(2,128)} %pre_ref.1, bf16[2,256,512]{2,1,0:T(8,128)(2,1)} %wv_hbm.1, bf16[2,256,512]{2,1,0:T(8,128)(2,1)} %wg_hbm.1, f32[31,2,512]{2,1,0:T(2,128)} %bitcast.1, f32[2,512]{1,0:T(2,128)} %ng_ref.1, f32[2,512]{1,0:T(2,128)} %ns_ref.1, ...), custom_call_target="tpu_custom_call" | custom-call | tf_op jit(solution)/shard_map/pallas_call | solution.py:645
  123.1 1.7 %copy.11 = bf16[320,512]{1,0:T(8,128)(2,1)} copy(bf16[320,512]{1,0:T(8,128)(2,1)} %shard_map.91) | data formatting | bytes 655360

commit v3 on v2

v3 whole, which is shorter than its diff:
```python
import jax
import jax.numpy as jnp
from jax import lax
from jax.experimental import pallas as pl
from jax.experimental.pallas import tpu as pltpu
from jax.sharding import PartitionSpec as P

D = 2048
CONV_WIDTH = 31
LAYERS = 2


EPSILON = 1e-06
LN_EPSILON = 1e-05


def passed_along(block, axis, distance):
    devices = range(lax.axis_size(axis))
    route = [(i - distance, i) for i in devices if i - distance in devices]
    return lax.ppermute(block, axis, route)


def local(tokens, pre_gain, w_value, w_gate, taps, norm_gain, norm_shift, w_out, post_gain):
    stream = tokens
    full_value, full_gate = (
        lax.all_gather(w_value, "sp", axis=1, tiled=True),
        lax.all_gather(w_gate, "sp", axis=1, tiled=True),
    )
    full_out = lax.all_gather(w_out, "sp", axis=2, tiled=True)
    for layer in range(LAYERS):
        whole = lax.all_gather(stream, "tp", axis=1, tiled=True)
        whole_f = whole.astype(jnp.float32)
        normed = (
            whole_f
            * lax.rsqrt(jnp.mean(whole_f * whole_f, -1, keepdims=True) + EPSILON)
            * pre_gain[layer]
        ).astype(jnp.bfloat16)
        value_mat = full_value[layer]
        gate_mat = full_gate[layer]
        out_mat = full_out[layer]
        value_proj = jnp.dot(normed, value_mat, preferred_element_type=jnp.float32)
        gate_proj = jnp.dot(normed, gate_mat, preferred_element_type=jnp.float32)
        glu_act = (value_proj * jax.nn.sigmoid(gate_proj)).astype(jnp.bfloat16)
        rows = glu_act.shape[0]
        fringe = passed_along(glu_act[rows - (CONV_WIDTH - 1) :], "sp", 1)
        padded = jnp.concatenate([fringe, glu_act], 0).astype(jnp.float32)
        conv_out = jnp.zeros(glu_act.shape, jnp.float32)
        for offset in range(CONV_WIDTH):
            conv_out = conv_out + taps[layer, offset] * padded[offset : offset + rows]
        row_sum, row_square = lax.psum(
            (jnp.sum(conv_out, -1, keepdims=True), jnp.sum(conv_out * conv_out, -1, keepdims=True)),
            "tp",
        )
        center = row_sum / D
        spread = jnp.maximum(row_square / D - center * center, 0.0)
        activated = jax.nn.silu(
            (conv_out - center) * lax.rsqrt(spread + LN_EPSILON) * norm_gain[layer]
            + norm_shift[layer]
        ).astype(jnp.bfloat16)
        terms = jnp.dot(activated, out_mat, preferred_element_type=jnp.float32)
        summed = lax.psum_scatter(terms.astype(jnp.bfloat16), "tp", scatter_dimension=1, tiled=True)
        projected = summed.astype(jnp.float32)
        out_square = lax.psum(jnp.sum(projected * projected, -1, keepdims=True), "tp")
        scale = lax.rsqrt(out_square / D + EPSILON)
        stream = (stream.astype(jnp.float32) + projected * scale * post_gain[layer]).astype(
            jnp.bfloat16
        )
    return stream


TILE = 64
PACK = 16
HALO = 32
OVER_X = ((True, True), (True, False))
FAR = (1, 2, 3)


def step(
    x_ref, pre_ref, wv_hbm, wg_hbm, taps_ref, ng_ref, ns_ref, wo_hbm, post_ref, out_ref,
    weight, other, whole, shared, stream, normed, fresh, kept, added, row_sums, row_moments, glu, conv, act,
    part_out, part_in, x_out, x_in, z_out, z_in, total, held,
    taps, gain, shift, pre_all, post_all, stat, stat_in, local_sem,
    zs, zr, ys, yr, gs, gr, fs, fr, hs, hr, ss, sr, ps, pr, xs, xr, bs, br, qs, qr,
):
    sp, tp = lax.axis_index("sp"), lax.axis_index("tp")
    rows, cols = x_ref.shape
    layers, units, nsp, ntp = 2, 6, 8, 4
    z, y = sp // 2, sp % 2
    zh, zl = z // 2, z % 2
    x, c = tp // 2, tp % 2
    plane = [z, zh * 2 + 1 - zl, (1 - zh) * 2 + zl, (1 - zh) * 2 + 1 - zl]
    partner = plane[1] * 2 + y
    beside, facing = (partner, tp), (z * 2 + 1 - y, tp)
    mate, across, diagonal = (sp, x * 2 + 1 - c), (sp, (1 - x) * 2 + c), (sp, (1 - x) * 2 + 1 - c)
    both, half, tiles = 2 * rows, cols // 2, rows // TILE
    mine = pl.ds(pl.multiple_of(zl * half, half), half)
    rest = pl.ds(pl.multiple_of((1 - zl) * half, half), half)
    depth, each = wv_hbm.shape[1], wo_hbm.shape[2]
    per = cols // each

    def copy(src, dst, send, recv, to):
        return pltpu.make_async_remote_copy(
            src_ref=src, dst_ref=dst, send_sem=send, recv_sem=recv, device_id=to,
            device_id_type=pl.DeviceIdType.MESH,
        )

    def took(b, sem):
        copy(b, b, sem, sem, mate).wait_recv()

    def left(b, sem):
        copy(b, b, sem, sem, mate).wait_send()

    def block(i, size=TILE):
        if isinstance(i, int):
            return pl.ds(i * size, size)
        return pl.ds(pl.multiple_of(i * size, size), size)

    def piece(u, slot):
        return weight.at[u, block(slot, depth)]

    def landing(u, k):
        return zr.at[u * 3 + k - 1]

    def along(u, k):
        p = piece(u, sp)
        src = p if k == 2 else other.at[u]
        return copy(src, p, zs.at[k - 1], landing(u, k), (plane[k] * 2 + y, tp))

    def own(u):
        for k in FAR:
            along(u, k).start()

    def sideways(u, k):
        p = piece(u, plane[k] * 2 + y)
        copy(p, p, ys.at[0], yr.at[u], facing).start()

    def relay(u, *ks):
        for k in ks:
            took(piece(u, plane[k] * 2 + y), landing(u, k))
            sideways(u, k)

    def relay_near(u):
        pl.when(zl == zh)(lambda: relay(u, 2))
        pl.when(zl != zh)(lambda: relay(u, 3))

    def relay_far(u):
        pl.when(zl == zh)(lambda: relay(u, 3))
        pl.when(zl != zh)(lambda: relay(u, 2))

    def arrive(u):
        took(weight.at[u, : 4 * depth], yr.at[u])

    here, there = zl * 4, (1 - zl) * 4
    opposite = (1 - x) * 2 + c
    upper, lower = pl.ds(0, rows // 2), pl.ds(rows // 2, rows // 2)
    full = pl.ds(0, rows)
    routes = dict(
        across=(here + tp, full, across, 0),
        beside_upper=(here + tp, upper, beside, 1),
        beside_lower=(here + tp, lower, beside, 2),
        mate=(here + tp, full, mate, 5),
        diagonal_upper=(there + tp, upper, across, 3),
        diagonal_lower=(there + tp, lower, across, 4),
        across_mate=(here + opposite, full, mate, 5),
        beside_mate=(there + tp, full, mate, 5),
        both_mate_upper=(there + opposite, upper, mate, 5),
        both_mate_lower=(there + opposite, lower, mate, 5),
    )

    def gather(name):
        t, part, to, k = routes[name]
        b = whole.at[t, part]
        copy(b, b, gs.at[0], gr.at[k], to).start()

    def came(name, t):
        took(whole.at[t, routes[name][1]], gr.at[routes[name][3]])

    def gather_start():
        for name in ("across", "beside_upper", "beside_lower", "mate"):
            gather(name)

    def gather_upper():
        came("beside_upper", there + tp)
        gather("diagonal_upper")

    def gather_lower():
        came("beside_lower", there + tp)
        gather("diagonal_lower")
        gather("beside_mate")

    def gather_across():
        came("across", here + opposite)
        gather("across_mate")

    def gather_last():
        came("diagonal_upper", there + opposite)
        gather("both_mate_upper")
        came("diagonal_lower", there + opposite)
        gather("both_mate_lower")

    def row_scale(square):
        return lax.rsqrt(square / (cols * ntp) + EPSILON)

    def norm():
        took(whole.at[0:4], gr.at[5])

        @pl.loop(0, 2 * tiles)
        def _(i):
            g, r = i // tiles * 4, block(i % tiles)
            square = jnp.zeros((TILE, 1), jnp.float32)
            for t in range(ntp):
                v = whole[g + t, r, :].astype(jnp.float32)
                square = square + jnp.sum(v * v, -1, keepdims=True)
            scale = row_scale(square)
            for t in range(ntp):
                v = whole[g + t, r, :].astype(jnp.float32)
                at = slice(t * cols, (t + 1) * cols)
                normed[block(i), at] = (v * scale * pre_ref[0:1, at]).astype(jnp.bfloat16)

    def project_kept(l, kind):
        w = weight[3 * l + kind]
        for part in (slice(0, rows), slice(rows, both)):
            kept[kind, part] = jnp.dot(normed[part], w, preferred_element_type=jnp.float32)

    pair_tp, pair_opposite = x * 2 + 1 - c, (1 - x) * 2 + 1 - c
    hand = dict(
        across=(here + tp, across, here + opposite, 0),
        beside=(here + tp, beside, there + tp, 2),
        diagonal=(there + tp, across, there + opposite, 4),
        across_mate=(here + opposite, mate, here + pair_opposite, 6),
        beside_mate=(there + tp, mate, there + pair_tp, 8),
        both_mate=(there + opposite, mate, there + pair_opposite, 10),
        mate=(here + tp, mate, here + pair_tp, 12),
    )

    def share(name, h):
        t, to, _, k = hand[name]
        b = shared.at[t, h]
        copy(b, b, fs.at[0], fr.at[k if name == "mate" else k + h], to).start()

    def shared_wait(name, h):
        if name == "mate":
            took(shared.at[here + pair_tp], fr.at[12])
        else:
            took(shared.at[hand[name][2], h], fr.at[hand[name][3] + h])

    def share_turn(name, h):
        shared_wait(name, h)
        if name == "beside":
            share("diagonal", h)
        share("both_mate" if name == "diagonal" else name + "_mate", h)

    def keep_old():
        @pl.loop(0, 2 * tiles)
        def _(i):
            g, r = i // tiles * 4, block(i % tiles)
            square = jnp.zeros((TILE, 128), jnp.float32)
            for t in range(ntp):
                v = whole[g + t, r, :].astype(jnp.float32)
                at = slice(t * cols, (t + 1) * cols)
                normed[block(i), at] = (v * pre_ref[1:2, at]).astype(jnp.bfloat16)
                for j in range(cols // 128):
                    w = v[:, j * 128 : (j + 1) * 128]
                    square = square + w * w
            row_sums[3, block(i), :] = square

    groups_of = dict(
        mate=(zl, x), across_mate=(zl, 1 - x), beside_mate=(1 - zl, x), both_mate=(1 - zl, 1 - x)
    )
    begun = set()

    def fold(v):
        out = v[:, :128]
        for j in range(1, each // 128):
            out = out + v[:, j * 128 : (j + 1) * 128]
        return out

    def prepare(name, h):
        q, column = groups_of[name]
        side = name in ("mate", "across_mate")
        start = ("sums", side) not in begun
        begun.add(("sums", side))
        at = slice(h * each, (h + 1) * each)

        @pl.loop(0, tiles)
        def _(i):
            r, to = block(i), block(q * tiles + i)
            sums = [jnp.zeros((TILE, 128), jnp.float32) if start else row_sums[n, to, :] for n in range(3)]
            for core in range(2):
                t = column * 2 + core
                v = shared[q * 4 + t, h, r, :].astype(jnp.float32)
                old = whole[q * 4 + t, r, at].astype(jnp.float32)
                w = v * post_all[t, 0:1, at]
                fresh[q * 4 + t, h, r, :] = (w * pre_all[t, 1:2, at]).astype(jnp.bfloat16)
                sums = [s + fold(p) for s, p in zip(sums, (v * v, old * w, w * w))]
            for n in range(3):
                row_sums[n, to, :] = sums[n]

    def multiply(name, h, kinds=(0, 1)):
        q, column = groups_of[name]
        side, to = name in ("mate", "across_mate"), block(q, rows)
        sums = []
        for kind in kinds:
            v = None
            for core in range(2):
                t = column * 2 + core
                w = weight[3 + kind, block(t * per + h, depth), :]
                p = jnp.dot(fresh[q * 4 + t, h], w, preferred_element_type=jnp.float32)
                v = p if v is None else v + p
            sums.append(v)
        for kind, v in zip(kinds, sums):
            start = (kind, side) not in begun
            begun.add((kind, side))
            added[kind, to, :] = v if start else added[kind, to, :] + v

    def scales(to):
        new, cross, square, old = [
            jnp.sum(row_sums[n, to, :], -1, keepdims=True) for n in range(4)
        ]
        s = row_scale(new)
        return s, row_scale(jnp.maximum(old + 2.0 * s * cross + s * s * square, 0.0))

    def gate_tile(l, i):
        to = block(i)
        value, gate = kept[0, to, :], kept[1, to, :]
        if l:
            s, n = scales(to)
            value = n * (value + s * added[0, to, :])
            gate = n * (gate + s * added[1, to, :])
        made = (value * jax.nn.sigmoid(gate)).astype(jnp.bfloat16)
        glu[l, i // tiles, pl.ds(HALO + i % tiles * TILE, TILE), :] = made

    def project(l):
        inner = tiles - 1
        for q in range(2):
            gate_tile(l, q * tiles + inner)
        halo_send(l, lambda h: h.start())
        for i in range(2 * inner):
            gate_tile(l, i + i // inner)

    def new_stream():
        @pl.loop(0, tiles)
        def _(i):
            r = block(i)
            s, _ = scales(block(zl * tiles + i))
            for h in range(per):
                at = slice(h * each, (h + 1) * each)
                v = shared[here + tp, h, r, :].astype(jnp.float32)
                old = whole[here + tp, r, at].astype(jnp.float32)
                stream[r, at] = (old + v * s * post_ref[0:1, at]).astype(jnp.bfloat16)

    tail, head = pl.ds(rows, HALO), pl.ds(0, HALO)

    def near_halo(l):
        return copy(glu.at[l, 0, tail], glu.at[l, y, head], hs.at[l, 0], hr.at[l, y], facing)

    def even_halo(l):
        return copy(glu.at[l, 1, tail], glu.at[l, 1, head], hs.at[l, 1], hr.at[l, 1], facing)

    def odd_halo(l):
        return copy(
            glu.at[l, 1, tail], glu.at[l, 0, head], hs.at[l, 1], hr.at[l, 0], ((z + 2) * 2, tp)
        )

    def halo_send(l, act_on):
        act_on(near_halo(l))
        pl.when(y == 0)(lambda: act_on(even_halo(l)))
        pl.when((y == 1) & (zh == 0))(lambda: act_on(odd_halo(l)))

    def halo_wait(l):
        pl.when((y == 1) | (zh == 1))(lambda: took(glu.at[l, 0, head], hr.at[l, 0]))
        took(glu.at[l, 1, head], hr.at[l, 1])

        @pl.when((y == 0) & (zh == 0))
        def _():
            glu[l, 0, :HALO] = jnp.zeros((HALO, half), jnp.bfloat16)

    peers = [mate, across, diagonal, beside]
    peers += [(partner, mate[1]), (partner, across[1]), (partner, diagonal[1])]

    def exchange(e):
        for j, to in enumerate(peers[: 3 if e == layers else 7]):
            copy(stat.at[e], stat_in.at[e, j], ss.at[e], sr.at[e], to).start()

    def inbox(e):
        return stat_in.at[e, 0 : 3 if e == layers else 7]

    def received(e):
        sums = stat[e]
        for j in range(3 if e == layers else 7):
            sums = sums + stat_in[e, j]
        return sums

    lane = lax.broadcasted_iota(jnp.int32, (PACK, 128), 1)
    groups = TILE // PACK

    def pick(sums, at):
        found = [
            jnp.sum(jnp.where(lane == at * groups + g, sums, 0.0), -1, keepdims=True)
            for g in range(groups)
        ]
        return jnp.concatenate(found, 0)

    def pack(sums, at, column):
        for g in range(groups):
            sums = jnp.where(lane == at * groups + g, column[g * PACK : (g + 1) * PACK], sums)
        return sums

    def convolve(l):
        first = HALO - (CONV_WIDTH - 1)

        def tile(q, i):
            r = pl.multiple_of(i * TILE, TILE)
            one = jnp.zeros((TILE, 128), jnp.float32)
            two = jnp.zeros((TILE, 128), jnp.float32)
            for j in range(half // 128):
                at = slice(j * 128, (j + 1) * 128)
                window = glu[l, q, pl.ds(r, TILE + HALO), at].astype(jnp.float32)
                acc = jnp.zeros((TILE, 128), jnp.float32)
                for s in range(8):
                    w = window if s == 0 else pltpu.roll(window, TILE + HALO - s, 0)
                    for k in range(CONV_WIDTH):
                        if (first + k) % 8 == s:
                            o = first + k - s
                            acc = acc + taps[l, k : k + 1, at] * w[o : o + TILE]
                conv[q, pl.ds(r, TILE), at] = acc
                one = one + acc
                two = two + acc * acc
            row_moments[0, block(q * tiles + i), :] = one
            row_moments[1, block(q * tiles + i), :] = two

        inner = tiles - 1
        pl.loop(0, 2 * inner)(lambda i: tile(i // inner, i % inner + 1))
        halo_wait(l)
        pl.loop(0, 2)(lambda q: tile(q, 0))
        sums = jnp.zeros((PACK, 128), jnp.float32)
        for i in range(2 * tiles):
            for n in range(2):
                sums = pack(sums, 2 * i + n, jnp.sum(row_moments[n, block(i), :], -1, keepdims=True))
        stat[l] = sums
        exchange(l)

    def moments(l):
        took(inbox(l), sr.at[l])

    def activate(l, q):
        sums = received(l)

        for i in range(tiles):
            at, r = q * tiles + i, block(i)
            center = pick(sums, 2 * at) / (cols * ntp)
            spread = jnp.maximum(pick(sums, 2 * at + 1) / (cols * ntp) - center * center, 0.0)
            v = (conv[q, r, :] - center) * lax.rsqrt(spread + LN_EPSILON)
            v = v * gain[l : l + 1, :] + shift[l : l + 1, :]
            act[q, r, :] = (v * jax.nn.sigmoid(v)).astype(jnp.bfloat16)

    quads = dict(D=(1 - zl, 1 - x), A=(zl, 1 - x), B=(1 - zl, x), O=(zl, x))
    names = list(quads)

    def term(l, quad, h, core):
        q, column = quads[quad]
        w = weight[3 * l + 2, block((column * 2 + core) * per + h, depth), :]
        return jnp.dot(act[q], w, preferred_element_type=jnp.float32).astype(jnp.bfloat16)

    def give(l, quad):
        i = names.index(quad)
        made = [term(l, quad, h, 1 - c) for h in range(per)]
        for h in range(per):
            part_out[l, i, h] = made[h]
        copy(part_out.at[l, i], part_in.at[l, i], ps.at[l], pr.at[l, i], mate).start()

    def joined(l, quad):
        i = names.index(quad)
        made = [term(l, quad, h, c).astype(jnp.float32) for h in range(per)]
        took(part_in.at[l, i], pr.at[l, i])
        return [made[h] + part_in[l, i, h].astype(jnp.float32) for h in range(per)]

    def pass_x(l, i, v):
        x_out[l, i] = v.astype(jnp.bfloat16)
        copy(x_out.at[l, i], x_in.at[l, i], xs.at[l], xr.at[l, i], across).start()

    def pass_z(l, i, v):
        z_out[l, i] = v.astype(jnp.bfloat16)
        copy(z_out.at[l, i], z_in.at[l, i], bs.at[l], br.at[l, i], beside).start()

    def move_on(l, quad):
        for h, v in enumerate(joined(l, quad)):
            if quad == "O":
                total[:, h * each : (h + 1) * each] = v
            elif (quad == "A" and OVER_X[l][h]) or (quad == "D" and OVER_X[l][h]):
                pass_x(l, h if quad == "D" else 2 + h, v)
            elif quad == "D" or (quad == "B" and not OVER_X[l][h]):
                pass_z(l, h if quad == "D" else 2 + h, v)
            else:
                held[h] = v

    def pass_held(l, h):
        if OVER_X[l][h]:
            took(x_in.at[l, h], xr.at[l, h])
            pass_z(l, 2 + h, held[h] + x_in[l, h].astype(jnp.float32))
        else:
            took(z_in.at[l, h], br.at[l, h])
            pass_x(l, 2 + h, held[h] + z_in[l, h].astype(jnp.float32))

    def steps(l, *todo):
        for name in todo:
            (give if name[0] == "g" else move_on)(l, name[1])

    def projected(l, h, r):
        at = slice(h * each, (h + 1) * each)
        p = total[r, at] + x_in[l, 2 + h, r, :].astype(jnp.float32)
        return (p + z_in[l, 2 + h, r, :].astype(jnp.float32)).astype(jnp.bfloat16)

    def landed(l, h):
        took(x_in.at[l, 2 + h], xr.at[l, 2 + h])
        took(z_in.at[l, 2 + h], br.at[l, 2 + h])

    def settle(h):
        landed(0, h)

        @pl.loop(0, tiles)
        def _(i):
            shared[here + tp, h, block(i), :] = projected(0, h, block(i))

        for name in ("across", "beside", "mate"):
            share(name, h)

    def finish():
        l = layers - 1
        for h in range(per):
            landed(l, h)

        def tile(i, sums):
            r = block(i)
            square = jnp.zeros((TILE, 1), jnp.float32)
            for h in range(per):
                p = projected(l, h, r).astype(jnp.float32)
                total[r, h * each : (h + 1) * each] = p
                square = square + jnp.sum(p * p, -1, keepdims=True)
            return pack(sums, i, square)

        sums = jnp.zeros((PACK, 128), jnp.float32)
        for i in range(tiles):
            sums = tile(i, sums)
        stat[layers] = sums
        exchange(layers)
        took(inbox(layers), sr.at[layers])
        sums = received(layers)
        for i in range(tiles):
            r = block(i)
            new = total[r, :] * row_scale(pick(sums, i)) * post_ref[l : l + 1, :]
            out_ref[r, :] = (stream[r, :].astype(jnp.float32) + new).astype(jnp.bfloat16)

    pltpu.make_async_copy(x_ref, whole.at[here + tp], local_sem.at[2]).start()
    for u in range(units):
        l, kind = divmod(u, 3)
        ref = (wv_hbm, wg_hbm, wo_hbm)[kind]
        for i, (part, to) in enumerate(((mine, piece(u, sp)), (rest, other.at[u]))):
            src = ref.at[l, part] if kind == 2 else ref.at[l, :, part]
            pltpu.make_async_copy(src, to, local_sem.at[i]).start()
    post_all[tp] = post_ref[...]
    for t in range(ntp):
        pre_all[t] = pre_ref[:, t * cols : (t + 1) * cols]
    for l in range(layers):
        taps[l] = taps_ref[:, l, mine]
        gain[l : l + 1] = ng_ref[l : l + 1, mine]
        shift[l : l + 1] = ns_ref[l : l + 1, mine]
    barrier = pltpu.get_barrier_semaphore()
    for i in range(1, nsp):
        pl.semaphore_signal(
            barrier, inc=1, device_id=(lax.rem(sp + i, nsp), tp),
            device_id_type=pl.DeviceIdType.MESH,
        )
    for i in range(1, ntp):
        for at in (sp, partner):
            pl.semaphore_signal(
                barrier, inc=1, device_id=(at, lax.rem(tp + i, ntp)),
                device_id_type=pl.DeviceIdType.MESH,
            )
    pl.semaphore_wait(barrier, nsp - 1 + 2 * (ntp - 1))
    for i in range(2):
        pltpu.make_async_copy(other, other, local_sem.at[i]).wait()
    pltpu.make_async_copy(x_ref, whole.at[here + tp], local_sem.at[2]).wait()

    def post_start():
        for to in (mate, across, diagonal):
            copy(post_ref, post_all.at[tp], qs.at[0], qr.at[0], to).start()

    def post_wait():
        took(post_all.at[0:3], qr.at[0])

    own(0)
    sideways(0, 0)
    gather_start()
    post_start()
    own(1)
    sideways(1, 0)
    sideways(2, 0)
    relay_near(0)
    relay(0, 1)
    relay_far(0)
    gather_upper()
    relay_near(1)
    gather_lower()
    relay(1, 1)
    relay_far(1)
    gather_across()
    own(2)
    sideways(3, 0)
    gather_last()
    norm()
    arrive(0)
    project_kept(0, 0)
    arrive(1)
    project_kept(0, 1)
    project(0)
    convolve(0)
    own(3)
    own(4)
    relay_near(2)
    relay(2, 1)
    relay_far(2)
    sideways(4, 0)
    moments(0)
    activate(0, 1 - zl)
    arrive(2)
    steps(0, "gD")
    activate(0, zl)
    steps(0, "gA", "mD", "gB", "mA", "gO", "mB", "mO")
    pass_held(0, 0)
    pass_held(0, 1)
    relay(3, 1, 2, 3)
    post_wait()
    keep_old()
    settle(0)
    relay(4, 1)
    settle(1)
    own(5)
    relay(4, 2, 3)
    sideways(5, 0)
    arrive(3)
    project_kept(1, 0)
    shared_wait("mate", 0)
    prepare("mate", 0)
    prepare("mate", 1)
    share_turn("beside", 0)
    share_turn("across", 0)
    shared_wait("across_mate", 0)
    prepare("across_mate", 0)
    shared_wait("beside_mate", 0)
    prepare("beside_mate", 0)
    share_turn("beside", 1)
    share_turn("across", 1)
    arrive(4)
    project_kept(1, 1)
    share_turn("diagonal", 0)
    multiply("mate", 0)
    multiply("mate", 1)
    multiply("across_mate", 0)
    multiply("beside_mate", 0)
    shared_wait("across_mate", 1)
    prepare("across_mate", 1)
    multiply("across_mate", 1)
    shared_wait("beside_mate", 1)
    prepare("beside_mate", 1)
    multiply("beside_mate", 1)
    shared_wait("both_mate", 0)
    prepare("both_mate", 0)
    multiply("both_mate", 0)
    share_turn("diagonal", 1)
    relay(5, 1)
    shared_wait("both_mate", 1)
    prepare("both_mate", 1)
    multiply("both_mate", 1)
    project(1)
    relay(5, 2, 3)
    convolve(1)
    new_stream()
    moments(1)
    activate(1, 1 - zl)
    arrive(5)
    steps(1, "gD")
    activate(1, zl)
    steps(1, "gA", "mD", "gB", "mA", "gO", "mB", "mO")
    pass_held(1, 1)
    pass_held(1, 0)
    finish()
    for k in FAR:
        left(other, zs.at[k - 1])
    left(weight.at[0:3], ys.at[0])
    left(whole.at[0:7], gs.at[0])
    left(shared.at[0:7], fs.at[0])
    left(post_all.at[0:3], qs.at[0])
    for l in range(layers):
        left(inbox(l), ss.at[l])
        left(part_out.at[l], ps.at[l])
        left(x_out.at[l, 0 : 2 + sum(OVER_X[l])], xs.at[l])
        left(z_out.at[l, 0 : 4 - sum(OVER_X[l])], bs.at[l])
        halo_send(l, lambda h: h.wait_send())
    left(inbox(layers), ss.at[layers])


def kernel_local(*args):
    tokens, pre_gain, w_value, w_gate, all_taps, norm_gain, norm_shift, w_out, post_gain = args
    rows, cols = tokens.shape
    layers, depth = w_value.shape[:2]
    each = w_out.shape[2]
    half, units = cols // 2, 3 * layers
    square = depth == half == each and depth % 128 == 0
    if rows % TILE or 4 * rows > PACK * 128 or layers != 2 or not square:
        return local(*args)
    vmem, hbm = pl.BlockSpec(memory_space=pltpu.VMEM), pl.BlockSpec(memory_space=pl.ANY)
    bf16, f32, dma = jnp.bfloat16, jnp.float32, pltpu.SemaphoreType.DMA
    return pl.pallas_call(
        step,
        out_shape=pltpu.VMEM((rows, cols), bf16),
        in_specs=[hbm, vmem, hbm, hbm, vmem, vmem, vmem, hbm, vmem],
        out_specs=vmem,
        scratch_shapes=[
            pltpu.VMEM((units, 8 * depth, half), bf16),
            pltpu.VMEM((units, depth, half), bf16),
            pltpu.VMEM((8, rows, cols), bf16),
            pltpu.VMEM((8, 2, rows, each), bf16),
            pltpu.VMEM((rows, cols), bf16),
            pltpu.VMEM((2 * rows, 4 * cols), bf16),
            pltpu.VMEM((8, 2, rows, each), bf16),
            pltpu.VMEM((2, 2 * rows, half), f32),
            pltpu.VMEM((2, 2 * rows, half), f32),
            pltpu.VMEM((4, 2 * rows, 128), f32),
            pltpu.VMEM((2, 2 * rows, 128), f32),
            pltpu.VMEM((layers, 2, HALO + rows, half), bf16),
            pltpu.VMEM((2, rows, half), f32),
            pltpu.VMEM((2, rows, half), bf16),
            pltpu.VMEM((layers, 4, 2, rows, each), bf16),
            pltpu.VMEM((layers, 4, 2, rows, each), bf16),
            pltpu.VMEM((layers, 4, rows, each), bf16),
            pltpu.VMEM((layers, 4, rows, each), bf16),
            pltpu.VMEM((layers, 4, rows, each), bf16),
            pltpu.VMEM((layers, 4, rows, each), bf16),
            pltpu.VMEM((rows, cols), f32),
            pltpu.VMEM((2, rows, each), f32),
            pltpu.VMEM((layers, CONV_WIDTH, half), f32),
            pltpu.VMEM((layers, half), f32),
            pltpu.VMEM((layers, half), f32),
            pltpu.VMEM((4, layers, cols), f32),
            pltpu.VMEM((4, layers, cols), f32),
            pltpu.VMEM((layers + 1, PACK, 128), f32),
            pltpu.VMEM((layers + 1, 7, PACK, 128), f32),
            dma((3,)),
            dma((3,)), dma((18,)),
            dma((1,)), dma((units,)),
            dma((1,)), dma((6,)),
            dma((1,)), dma((13,)),
            dma((layers, 2)), dma((layers, 2)),
            dma((layers + 1,)), dma((layers + 1,)),
            dma((layers,)), dma((layers, 4)),
            dma((layers,)), dma((layers, 4)),
            dma((layers,)), dma((layers, 4)),
            dma((1,)), dma((1,)),
        ],
        compiler_params=pltpu.CompilerParams(
            collective_id=0, has_side_effects=True, vmem_limit_bytes=56 * 1024 * 1024
        ),
    )(
        tokens, pre_gain, w_value, w_gate, jnp.swapaxes(all_taps, 0, 1), norm_gain, norm_shift, w_out,
        post_gain,
    )


def solution(mesh):
    nsp, ntp = mesh.shape["sp"], mesh.shape["tp"]
    body = kernel_local if nsp == 8 and ntp == 4 else local
    placed = (
        P("sp", "tp"),
        P(),
        P(None, "sp", "tp"),
        P(None, "sp", "tp"),
        P(None, None, "tp"),
        P(None, "tp"),
        P(None, "tp"),
        P(None, "tp", "sp"),
        P(None, "tp"),
    )
    return jax.shard_map(
        body, mesh=mesh, in_specs=placed, out_specs=P("sp", "tp"), check_vma=False
    )
```

time: 126 us -> 117 us (0.929); the launches traced: 125 us -> 117 us
  Pallas kernels: 123 us -> 116 us
    pallas_call x1, Pallas kernels: 123 us -> 116 us  [kernel_local(): pl.pallas_call(step, out_shape=pltpu.VMEM((rows, cols), bf16), in_specs=[...]
where the time goes in v3:
time: 117 us
  Pallas kernels  116 us (99%)
    pallas_call x1, Pallas kernels, kernel_local(): pl.pallas_call(step, out_shape=pltpu.VMEM((rows, cols), bf16), in_specs=[...  116 us

profile of v3, /device:TPU:0, one launch (start us, length us, event | category | flops | bytes accessed | tf_op | source)
XLA Modules:
  0.0 117.2 jit_solution(13934856544273936685)
XLA Ops:
  0.0 116.5 %shard_map.91 = bf16[320,512]{1,0:T(8,128)(2,1)S(1)} custom-call(bf16[320,512]{1,0:T(8,128)(2,1)} %x_ref.1, f32[2,2048]{1,0:T(2,128)} %pre_ref.1, bf16[2,256,512]{2,1,0:T(8,128)(2,1)} %wv_hbm.1, bf16[2,256,512]{2,1,0:T(8,128)(2,1)} %wg_hbm.1, f32[31,2,512]{2,1,0:T(2,128)} %bitcast.1, f32[2,512]{1,0:T(2,128)} %ng_ref.1, f32[2,512]{1,0:T(2,128)} %ns_ref.1, ...), custom_call_target="tpu_custom_call" | custom-call | tf_op jit(solution)/shard_map/pallas_call | solution.py:714
  116.5 0.7 copy.11

commit v4 on v3

--- a/solution.py
+++ b/solution.py
@@ -73,6 +73,7 @@
 HALO = 32
 OVER_X = ((True, True), (True, False))
 FAR = (1, 2, 3)
+SPLIT = 3
 
 
 def step(
@@ -115,37 +116,60 @@
             return pl.ds(i * size, size)
         return pl.ds(pl.multiple_of(i * size, size), size)
 
+    def parts(u):
+        return (0, 1) if u < SPLIT else (0,)
+
     def piece(u, slot):
         return weight.at[u, block(slot, depth)]
 
-    def landing(u, k):
-        return zr.at[u * 3 + k - 1]
-
-    def along(u, k):
-        p = piece(u, sp)
-        src = p if k == 2 else other.at[u]
-        return copy(src, p, zs.at[k - 1], landing(u, k), (plane[k] * 2 + y, tp))
+    def part_of(u, slot, part):
+        if u >= SPLIT:
+            return piece(u, slot)
+        return weight.at[u, block(slot * 2 + part, depth // 2)]
+
+    def landing(u, k, part):
+        if u < SPLIT:
+            return zr.at[(u * 3 + k - 1) * 2 + part]
+        return zr.at[SPLIT * 3 + u * 3 + k - 1]
+
+    def along(u, k, part):
+        p = part_of(u, sp, part)
+        src = other.at[u, block(part, depth // len(parts(u)))]
+        to = (plane[k] * 2 + y, tp)
+        copy(p if k == 2 else src, p, zs.at[k - 1], landing(u, k, part), to).start()
 
     def own(u):
-        for k in FAR:
-            along(u, k).start()
-
-    def sideways(u, k):
-        p = piece(u, plane[k] * 2 + y)
+        for part in parts(u):
+            for k in FAR:
+                along(u, k, part)
+
+    def sideways(u, k, part=0):
+        p = part_of(u, plane[k] * 2 + y, part)
         copy(p, p, ys.at[0], yr.at[u], facing).start()
 
-    def relay(u, *ks):
-        for k in ks:
-            took(piece(u, plane[k] * 2 + y), landing(u, k))
-            sideways(u, k)
-
-    def relay_near(u):
-        pl.when(zl == zh)(lambda: relay(u, 2))
-        pl.when(zl != zh)(lambda: relay(u, 3))
-
-    def relay_far(u):
-        pl.when(zl == zh)(lambda: relay(u, 3))
-        pl.when(zl != zh)(lambda: relay(u, 2))
+    def own_sideways(u):
+        for part in parts(u):
+            sideways(u, 0, part)
+
+    def relay(u, k, part):
+        took(part_of(u, plane[k] * 2 + y, part), landing(u, k, part))
+        sideways(u, k, part)
+
+    def relay_near(u, part=0):
+        pl.when(zl == zh)(lambda: relay(u, 2, part))
+        pl.when(zl != zh)(lambda: relay(u, 3, part))
+
+    def relay_far(u, part=0):
+        pl.when(zl == zh)(lambda: relay(u, 3, part))
+        pl.when(zl != zh)(lambda: relay(u, 2, part))
+
+    def relay_beside(u, part=0):
+        relay(u, 1, part)
+
+    def relay_all(u, part=0):
+        relay_near(u, part)
+        relay_beside(u, part)
+        relay_far(u, part)
 
     def arrive(u):
         took(weight.at[u, : 4 * depth], yr.at[u])
@@ -406,9 +430,9 @@
             sums = jnp.where(lane == at * groups + g, column[g * PACK : (g + 1) * PACK], sums)
         return sums
 
-    def convolve(l):
-        first = HALO - (CONV_WIDTH - 1)
-
+    first = HALO - (CONV_WIDTH - 1)
+
+    def convolver(l):
         def tile(q, i):
             r = pl.multiple_of(i * TILE, TILE)
             one = jnp.zeros((TILE, 128), jnp.float32)
@@ -429,8 +453,14 @@
             row_moments[0, block(q * tiles + i), :] = one
             row_moments[1, block(q * tiles + i), :] = two
 
-        inner = tiles - 1
+        return tile
+
+    def convolve_inner(l):
+        tile, inner = convolver(l), tiles - 1
         pl.loop(0, 2 * inner)(lambda i: tile(i // inner, i % inner + 1))
+
+    def convolve_first(l):
+        tile = convolver(l)
         halo_wait(l)
         pl.loop(0, 2)(lambda q: tile(q, 0))
         sums = jnp.zeros((PACK, 128), jnp.float32)
@@ -590,23 +620,23 @@
         took(post_all.at[0:3], qr.at[0])
 
     own(0)
-    sideways(0, 0)
+    own_sideways(0)
     gather_start()
     post_start()
     own(1)
-    sideways(1, 0)
-    sideways(2, 0)
-    relay_near(0)
-    relay(0, 1)
-    relay_far(0)
+    own_sideways(1)
+    own_sideways(2)
+    relay_all(0)
+    relay_all(0, 1)
     gather_upper()
     relay_near(1)
     gather_lower()
-    relay(1, 1)
+    relay_beside(1)
     relay_far(1)
+    relay_all(1, 1)
     gather_across()
     own(2)
-    sideways(3, 0)
+    own_sideways(3)
     gather_last()
     norm()
     arrive(0)
@@ -614,13 +644,13 @@
     arrive(1)
     project_kept(0, 1)
     project(0)
-    convolve(0)
+    relay_all(2)
+    convolve_inner(0)
+    convolve_first(0)
     own(3)
     own(4)
-    relay_near(2)
-    relay(2, 1)
-    relay_far(2)
-    sideways(4, 0)
+    relay_all(2, 1)
+    own_sideways(4)
     moments(0)
     activate(0, 1 - zl)
     arrive(2)
@@ -628,16 +658,17 @@
     activate(0, zl)
     steps(0, "gA", "mD", "gB", "mA", "gO", "mB", "mO")
     pass_held(0, 0)
+    relay_near(3)
+    relay_beside(3)
     pass_held(0, 1)
-    relay(3, 1, 2, 3)
+    relay_far(3)
     post_wait()
     keep_old()
     settle(0)
-    relay(4, 1)
+    relay_all(4)
     settle(1)
     own(5)
-    relay(4, 2, 3)
-    sideways(5, 0)
+    own_sideways(5)
     arrive(3)
     project_kept(1, 0)
     shared_wait("mate", 0)
@@ -668,13 +699,15 @@
     prepare("both_mate", 0)
     multiply("both_mate", 0)
     share_turn("diagonal", 1)
-    relay(5, 1)
+    relay_near(5)
     shared_wait("both_mate", 1)
     prepare("both_mate", 1)
     multiply("both_mate", 1)
     project(1)
-    relay(5, 2, 3)
-    convolve(1)
+    relay_beside(5)
+    relay_far(5)
+    convolve_inner(1)
+    convolve_first(1)
     new_stream()
     moments(1)
     activate(1, 1 - zl)
@@ -747,7 +780,7 @@
             pltpu.VMEM((layers + 1, PACK, 128), f32),
             pltpu.VMEM((layers + 1, 7, PACK, 128), f32),
             dma((3,)),
-            dma((3,)), dma((18,)),
+            dma((3,)), dma((18 + 3 * SPLIT,)),
             dma((1,)), dma((units,)),
             dma((1,)), dma((6,)),
             dma((1,)), dma((13,)),

time: 117 us -> 114 us (0.974)
  Pallas kernels: 116 us -> 113 us
    pallas_call x1, Pallas kernels: 116 us -> 113 us  [kernel_local(): pl.pallas_call(step, out_shape=pltpu.VMEM((rows, cols), bf16), in_specs=[...]
where the time goes in v4:
time: 114 us
  Pallas kernels  113 us (99%)
    pallas_call x1, Pallas kernels, kernel_local(): pl.pallas_call(step, out_shape=pltpu.VMEM((rows, cols), bf16), in_specs=[...  113 us

profile of v4, /device:TPU:0, one launch (start us, length us, event | category | flops | bytes accessed | tf_op | source)
XLA Modules:
  0.0 113.7 jit_solution(6103190084145761218)
XLA Ops:
  0.0 113.0 %shard_map.91 = bf16[320,512]{1,0:T(8,128)(2,1)S(1)} custom-call(bf16[320,512]{1,0:T(8,128)(2,1)} %x_ref.1, f32[2,2048]{1,0:T(2,128)} %pre_ref.1, bf16[2,256,512]{2,1,0:T(8,128)(2,1)} %wv_hbm.1, bf16[2,256,512]{2,1,0:T(8,128)(2,1)} %wg_hbm.1, f32[31,2,512]{2,1,0:T(2,128)} %bitcast.1, f32[2,512]{1,0:T(2,128)} %ng_ref.1, f32[2,512]{1,0:T(2,128)} %ns_ref.1, ...), custom_call_target="tpu_custom_call" | custom-call | tf_op jit(solution)/shard_map/pallas_call | solution.py:747
  113.0 0.7 copy.11

commit v5 on v4

--- a/solution.py
+++ b/solution.py
@@ -73,11 +73,12 @@
 HALO = 32
 OVER_X = ((True, True), (True, False))
 FAR = (1, 2, 3)
-SPLIT = 3
+PARTS = (2, 2, 4, 1, 1, 2)
 
 
 def step(
-    x_ref, pre_ref, wv_hbm, wg_hbm, taps_ref, ng_ref, ns_ref, wo_hbm, post_ref, out_ref,
+    x_ref, pre_hbm, wv_hbm, wg_hbm, taps_hbm, ng_hbm, ns_hbm, wo_hbm, post_hbm, out_ref,
+    pre_ref, taps_ref, ng_ref, ns_ref, post_ref,
     weight, other, whole, shared, stream, normed, fresh, kept, added, row_sums, row_moments, glu, conv, act,
     part_out, part_in, x_out, x_in, z_out, z_in, total, held,
     taps, gain, shift, pre_all, post_all, stat, stat_in, local_sem,
@@ -117,29 +118,25 @@
         return pl.ds(pl.multiple_of(i * size, size), size)
 
     def parts(u):
-        return (0, 1) if u < SPLIT else (0,)
+        return range(PARTS[u])
 
     def piece(u, slot):
         return weight.at[u, block(slot, depth)]
 
     def part_of(u, slot, part):
-        if u >= SPLIT:
-            return piece(u, slot)
-        return weight.at[u, block(slot * 2 + part, depth // 2)]
+        return weight.at[u, block(slot * PARTS[u] + part, depth // PARTS[u])]
 
     def landing(u, k, part):
-        if u < SPLIT:
-            return zr.at[(u * 3 + k - 1) * 2 + part]
-        return zr.at[SPLIT * 3 + u * 3 + k - 1]
+        return zr.at[3 * (sum(PARTS[:u]) + part) + k - 1]
 
     def along(u, k, part):
         p = part_of(u, sp, part)
-        src = other.at[u, block(part, depth // len(parts(u)))]
+        src = other.at[u, block(part, depth // PARTS[u])]
         to = (plane[k] * 2 + y, tp)
         copy(p if k == 2 else src, p, zs.at[k - 1], landing(u, k, part), to).start()
 
-    def own(u):
-        for part in parts(u):
+    def own(u, *some):
+        for part in some or parts(u):
             for k in FAR:
                 along(u, k, part)
 
@@ -166,10 +163,11 @@
     def relay_beside(u, part=0):
         relay(u, 1, part)
 
-    def relay_all(u, part=0):
-        relay_near(u, part)
-        relay_beside(u, part)
-        relay_far(u, part)
+    def relay_all(u, *some):
+        for part in some or (0,):
+            relay_near(u, part)
+            relay_beside(u, part)
+            relay_far(u, part)
 
     def arrive(u):
         took(weight.at[u, : 4 * depth], yr.at[u])
@@ -581,20 +579,6 @@
             new = total[r, :] * row_scale(pick(sums, i)) * post_ref[l : l + 1, :]
             out_ref[r, :] = (stream[r, :].astype(jnp.float32) + new).astype(jnp.bfloat16)
 
-    pltpu.make_async_copy(x_ref, whole.at[here + tp], local_sem.at[2]).start()
-    for u in range(units):
-        l, kind = divmod(u, 3)
-        ref = (wv_hbm, wg_hbm, wo_hbm)[kind]
-        for i, (part, to) in enumerate(((mine, piece(u, sp)), (rest, other.at[u]))):
-            src = ref.at[l, part] if kind == 2 else ref.at[l, :, part]
-            pltpu.make_async_copy(src, to, local_sem.at[i]).start()
-    post_all[tp] = post_ref[...]
-    for t in range(ntp):
-        pre_all[t] = pre_ref[:, t * cols : (t + 1) * cols]
-    for l in range(layers):
-        taps[l] = taps_ref[:, l, mine]
-        gain[l : l + 1] = ng_ref[l : l + 1, mine]
-        shift[l : l + 1] = ns_ref[l : l + 1, mine]
     barrier = pltpu.get_barrier_semaphore()
     for i in range(1, nsp):
         pl.semaphore_signal(
@@ -607,25 +591,63 @@
                 barrier, inc=1, device_id=(at, lax.rem(tp + i, ntp)),
                 device_id_type=pl.DeviceIdType.MESH,
             )
+    small = [
+        pltpu.make_async_copy(src, dst, local_sem.at[units + 1 + i])
+        for i, (src, dst) in enumerate((
+            (post_hbm, post_ref), (pre_hbm, pre_ref), (taps_hbm, taps_ref), (ng_hbm, ng_ref),
+            (ns_hbm, ns_ref),
+        ))
+    ]
+    tokens = pltpu.make_async_copy(x_ref, whole.at[here + tp], local_sem.at[units])
+    for u in range(units):
+        l, kind = divmod(u, 3)
+        ref = (wv_hbm, wg_hbm, wo_hbm)[kind]
+        for part, to in ((rest, other.at[u]), (mine, piece(u, sp))):
+            src = ref.at[l, part] if kind == 2 else ref.at[l, :, part]
+            pltpu.make_async_copy(src, to, local_sem.at[u]).start()
+        if u == 0:
+            tokens.start()
+            small[0].start()
+    for s in small[1:]:
+        s.start()
     pl.semaphore_wait(barrier, nsp - 1 + 2 * (ntp - 1))
-    for i in range(2):
-        pltpu.make_async_copy(other, other, local_sem.at[i]).wait()
-    pltpu.make_async_copy(x_ref, whole.at[here + tp], local_sem.at[2]).wait()
+
+    def fetched(u):
+        pltpu.make_async_copy(other.at[0:2], other.at[0:2], local_sem.at[u]).wait()
+
+    def set_up():
+        for s in small[1:]:
+            s.wait()
+        for t in range(ntp):
+            pre_all[t] = pre_ref[:, t * cols : (t + 1) * cols]
+        for l in range(layers):
+            taps[l] = taps_ref[:, l, mine]
+            gain[l : l + 1] = ng_ref[l : l + 1, mine]
+            shift[l : l + 1] = ns_ref[l : l + 1, mine]
 
     def post_start():
+        small[0].wait()
+        post_all[tp] = post_ref[...]
         for to in (mate, across, diagonal):
             copy(post_ref, post_all.at[tp], qs.at[0], qr.at[0], to).start()
 
     def post_wait():
         took(post_all.at[0:3], qr.at[0])
 
+    fetched(0)
     own(0)
     own_sideways(0)
+    tokens.wait()
     gather_start()
-    post_start()
+    fetched(1)
     own(1)
     own_sideways(1)
+    fetched(2)
     own_sideways(2)
+    post_start()
+    set_up()
+    for u in range(3, units):
+        fetched(u)
     relay_all(0)
     relay_all(0, 1)
     gather_upper()
@@ -635,7 +657,7 @@
     relay_far(1)
     relay_all(1, 1)
     gather_across()
-    own(2)
+    own(2, 0, 1, 2)
     own_sideways(3)
     gather_last()
     norm()
@@ -644,30 +666,28 @@
     arrive(1)
     project_kept(0, 1)
     project(0)
-    relay_all(2)
+    own(2, 3)
+    relay_all(2, 0, 1)
     convolve_inner(0)
+    relay_all(2, 2)
     convolve_first(0)
     own(3)
     own(4)
-    relay_all(2, 1)
+    relay_all(2, 3)
     own_sideways(4)
     moments(0)
     activate(0, 1 - zl)
+    activate(0, zl)
     arrive(2)
-    steps(0, "gD")
-    activate(0, zl)
-    steps(0, "gA", "mD", "gB", "mA", "gO", "mB", "mO")
+    steps(0, "gD", "gA", "mD", "gB", "mA", "gO", "mB", "mO")
     pass_held(0, 0)
-    relay_near(3)
-    relay_beside(3)
     pass_held(0, 1)
-    relay_far(3)
+    relay_all(3)
     post_wait()
     keep_old()
     settle(0)
     relay_all(4)
     settle(1)
-    own(5)
     own_sideways(5)
     arrive(3)
     project_kept(1, 0)
@@ -675,12 +695,14 @@
     prepare("mate", 0)
     prepare("mate", 1)
     share_turn("beside", 0)
+    own(5, 0)
     share_turn("across", 0)
     shared_wait("across_mate", 0)
     prepare("across_mate", 0)
     shared_wait("beside_mate", 0)
     prepare("beside_mate", 0)
     share_turn("beside", 1)
+    own(5, 1)
     share_turn("across", 1)
     arrive(4)
     project_kept(1, 1)
@@ -699,22 +721,20 @@
     prepare("both_mate", 0)
     multiply("both_mate", 0)
     share_turn("diagonal", 1)
-    relay_near(5)
+    relay_all(5)
     shared_wait("both_mate", 1)
     prepare("both_mate", 1)
     multiply("both_mate", 1)
     project(1)
-    relay_beside(5)
-    relay_far(5)
     convolve_inner(1)
+    relay_all(5, 1)
     convolve_first(1)
     new_stream()
     moments(1)
     activate(1, 1 - zl)
+    activate(1, zl)
     arrive(5)
-    steps(1, "gD")
-    activate(1, zl)
-    steps(1, "gA", "mD", "gB", "mA", "gO", "mB", "mO")
+    steps(1, "gD", "gA", "mD", "gB", "mA", "gO", "mB", "mO")
     pass_held(1, 1)
     pass_held(1, 0)
     finish()
@@ -747,9 +767,14 @@
     return pl.pallas_call(
         step,
         out_shape=pltpu.VMEM((rows, cols), bf16),
-        in_specs=[hbm, vmem, hbm, hbm, vmem, vmem, vmem, hbm, vmem],
+        in_specs=[hbm] * 9,
         out_specs=vmem,
         scratch_shapes=[
+            pltpu.VMEM((layers, 4 * cols), f32),
+            pltpu.VMEM((CONV_WIDTH, layers, cols), f32),
+            pltpu.VMEM((layers, cols), f32),
+            pltpu.VMEM((layers, cols), f32),
+            pltpu.VMEM((layers, cols), f32),
             pltpu.VMEM((units, 8 * depth, half), bf16),
             pltpu.VMEM((units, depth, half), bf16),
             pltpu.VMEM((8, rows, cols), bf16),
@@ -779,8 +804,8 @@
             pltpu.VMEM((4, layers, cols), f32),
             pltpu.VMEM((layers + 1, PACK, 128), f32),
             pltpu.VMEM((layers + 1, 7, PACK, 128), f32),
-            dma((3,)),
-            dma((3,)), dma((18 + 3 * SPLIT,)),
+            dma((units + 6,)),
+            dma((3,)), dma((3 * sum(PARTS),)),
             dma((1,)), dma((units,)),
             dma((1,)), dma((6,)),
             dma((1,)), dma((13,)),

time: 114 us -> 113 us (level)
  no operation moved by 1% of the time
where the time goes in v5:
time: 113 us
  Pallas kernels  112 us (99%)
    pallas_call x1, Pallas kernels, kernel_local(): pl.pallas_call(step, out_shape=pltpu.VMEM((rows, cols), bf16), in_specs=[...  112 us

profile of v5, /device:TPU:0, one launch (start us, length us, event | category | flops | bytes accessed | tf_op | source)
XLA Modules:
  0.0 112.7 jit_solution(5874681044569555417)
XLA Ops:
  0.0 111.9 %shard_map.91 = bf16[320,512]{1,0:T(8,128)(2,1)S(1)} custom-call(bf16[320,512]{1,0:T(8,128)(2,1)} %x_ref.1, f32[2,2048]{1,0:T(2,128)} %pre_hbm.1, bf16[2,256,512]{2,1,0:T(8,128)(2,1)} %wv_hbm.1, bf16[2,256,512]{2,1,0:T(8,128)(2,1)} %wg_hbm.1, f32[31,2,512]{2,1,0:T(2,128)} %bitcast.1, f32[2,512]{1,0:T(2,128)} %ng_hbm.1, f32[2,512]{1,0:T(2,128)} %ns_hbm.1, ...), custom_call_target="tpu_custom_call" | custom-call | tf_op jit(solution)/shard_map/pallas_call | solution.py:767
  111.9 0.7 copy.11
